TPU v7x, 768 devices: a whole 4x8x12 slice. The times are simulated.
768 devices in a mesh: sp: 96 (over z, y), tp: 8 (over x, core).
Axes of the slice: x: 4, y: 8, z: 12, core: 2. Of those that a mesh axis runs over, the one named last changes fastest.
Arguments:
- tokens: bfloat16 [24576, 2048], P('sp'), may hold values from -72 to 72
- query_weight: bfloat16 [3, 2048, 1024], P(None, None, 'tp'), may hold values from -0.125 to 0.125
- key_weight: bfloat16 [3, 2048, 1024], P(None, None, 'tp'), may hold values from -0.125 to 0.125
- value_weight: bfloat16 [3, 2048, 1024], P(None, None, 'tp'), may hold values from -0.125 to 0.125
- out_weight: bfloat16 [1024, 2048], P(None, 'tp'), may hold values from -2 to 2
Outputs:
- mixed: bfloat16 [24576, 2048], P('sp', 'tp')
All inputs are finite; a program needn't handle non-finite values.
Results may differ from a plain program's by a relative error of at most 0.012.
Values may be sent and summed in bfloat16 or wider, within the bound.
No kernel may reach another device: no remote copies, remote signals or barrier semaphores. Data moves between devices by JAX's collectives and lax.ppermute only.
A program may use at most 64 MiB of HBM per device.

v0:
```python
import math

import jax
import jax.numpy as jnp
from jax import lax
from jax.sharding import PartitionSpec as P

HEAD_DIM = 64
SIDE_STEPS = 64
MIDDLE_DILATION = 4
FAR_DILATION = 16


def with_halo(block, sides, width):
    for axis, dim in sides:
        count = lax.axis_size(axis)
        forward = [(i, i + 1) for i in range(count - 1)]
        backward = [(target, source) for source, target in forward]
        low = lax.ppermute(
            lax.slice_in_dim(block, block.shape[dim] - width, None, axis=dim), axis, forward
        )
        high = lax.ppermute(lax.slice_in_dim(block, 0, width, axis=dim), axis, backward)
        block = jnp.concatenate([low, block, high], axis=dim)
    return block


def shifted(block, axis, distance):
    devices = range(lax.axis_size(axis))
    route = [(i - distance, i) for i in devices if i - distance in devices]
    return lax.ppermute(block, axis, route)


def in_order(pieces, dim):
    pieces = jnp.moveaxis(pieces, 0, dim)
    lengths = pieces.shape
    return pieces.reshape(*lengths[:dim], lengths[dim] * lengths[dim + 1], *lengths[dim + 2 :])


def copy_for_each(value, axis):
    size = lax.axis_size(axis)
    return lax.all_to_all(
        jnp.broadcast_to(value[None], (size, *value.shape)), axis, 0, 0, tiled=True
    )


def collect(value, axis, dim):
    return in_order(copy_for_each(value, axis), dim)


def rotate(projected, offset_pos):
    length, columns = projected.shape
    heads = columns // HEAD_DIM
    half = HEAD_DIM // 2
    positions = (offset_pos + jnp.arange(length)).astype(jnp.float32)
    inverse = 1.0 / 10000.0 ** (jnp.arange(half, dtype=jnp.float32) * 2.0 / HEAD_DIM)
    angles = positions[:, None] * inverse[None, :]
    angles = jnp.concatenate([angles, angles], axis=-1)
    cosine_table = jnp.cos(angles)[:, None, :]
    sine = jnp.sin(angles)[:, None, :]
    shaped = projected.reshape(length, heads, HEAD_DIM)
    turned = jnp.concatenate([-shaped[..., half:], shaped[..., :half]], axis=-1)
    return (shaped * cosine_table + turned * sine).reshape(length, columns)


def banded(queries, key_ext, value_ext, dilation, offset_pos, seq_len):
    length, columns = queries.shape
    heads = columns // HEAD_DIM
    class_len = length // dilation
    block_len = math.gcd(SIDE_STEPS, class_len)
    blocks = class_len // block_len
    extra = 2 * SIDE_STEPS // block_len
    query_blocks = queries.reshape(blocks, block_len, dilation, heads, HEAD_DIM)
    key_blocks = key_ext.reshape(blocks + extra, block_len, dilation, heads, HEAD_DIM)
    value_blocks = value_ext.reshape(blocks + extra, block_len, dilation, heads, HEAD_DIM)
    key_win = jnp.concatenate(
        [key_blocks[shift_idx : shift_idx + blocks] for shift_idx in range(extra + 1)], axis=1
    )
    value_win = jnp.concatenate(
        [value_blocks[shift_idx : shift_idx + blocks] for shift_idx in range(extra + 1)], axis=1
    )
    scores = jnp.einsum(
        "bqrhe,bkrhe->brhqk", query_blocks, key_win, preferred_element_type=jnp.float32
    )
    scores = scores * HEAD_DIM ** (-0.5)
    width_keys = key_win.shape[1]
    relative = jnp.arange(width_keys)[None, :] - jnp.arange(block_len)[:, None]
    within = (relative >= 0) & (relative <= 2 * SIDE_STEPS)
    key_rows = jnp.arange(blocks)[:, None] * block_len + jnp.arange(width_keys)[None, :]
    spots = (
        offset_pos
        - SIDE_STEPS * dilation
        + dilation * key_rows[:, :, None]
        + jnp.arange(dilation)[None, None, :]
    )
    inside = (spots >= 0) & (spots < seq_len)
    allowed = within[None, None, None] & jnp.transpose(inside, (0, 2, 1))[:, :, None, None, :]
    scores = jnp.where(allowed, scores, -1e30)
    row_max = jnp.max(scores, axis=-1, keepdims=True)
    expo = jnp.exp(scores - row_max)
    denom = jnp.sum(expo, axis=-1)
    probs = expo.astype(jnp.bfloat16)
    summed = jnp.einsum("brhqk,bkrhe->bqrhe", probs, value_win, preferred_element_type=jnp.float32)
    group_out = summed / jnp.transpose(denom, (0, 3, 1, 2))[..., None]
    log_sum = row_max[..., 0] + jnp.log(denom)
    log_sum = jnp.transpose(log_sum, (0, 3, 1, 2)).reshape(length, heads)
    return (group_out.reshape(length, columns), log_sum)


def per_device(tokens, query_weight, key_weight, value_weight, out_weight):
    length = tokens.shape[0]
    offset_pos = lax.axis_index("sp") * length
    seq_len = lax.axis_size("sp") * length
    group_dilations = (1, MIDDLE_DILATION, FAR_DILATION)
    query_list = []
    pairs = []
    for group_idx in range(3):
        queries = rotate(
            jnp.dot(tokens, query_weight[group_idx], preferred_element_type=jnp.float32), offset_pos
        )
        keys_here = rotate(
            jnp.dot(tokens, key_weight[group_idx], preferred_element_type=jnp.float32), offset_pos
        )
        values_here = jnp.dot(tokens, value_weight[group_idx], preferred_element_type=jnp.float32)
        query_list.append(queries.astype(jnp.bfloat16))
        pairs.append(
            jnp.stack([keys_here.astype(jnp.bfloat16), values_here.astype(jnp.bfloat16)], axis=0)
        )
    middle_span_length = SIDE_STEPS * MIDDLE_DILATION
    joined = with_halo(
        jnp.concatenate([pairs[0], pairs[1]], axis=0), (("sp", 1),), middle_span_length
    )
    first_ext = joined[
        :2, middle_span_length - SIDE_STEPS : middle_span_length + length + SIDE_STEPS
    ]
    middle_ext = joined[2:]
    far_span_length = SIDE_STEPS * FAR_DILATION
    needed = -(-far_span_length // length)
    lower_list = []
    upper_list = []
    for distance in range(1, needed + 1):
        for direction in (1, -1):
            arrived = shifted(pairs[2], "sp", direction * distance)
            if direction > 0:
                lower_list.append(arrived)
            else:
                upper_list.append(arrived)
    lower_blocks = jnp.stack(lower_list, axis=0)
    upper_blocks = jnp.stack(upper_list, axis=0)
    columns = pairs[2].shape[2]
    lower_flat = jnp.moveaxis(lower_blocks[::-1], 0, 1).reshape(2, needed * length, columns)
    upper_flat = jnp.moveaxis(upper_blocks, 0, 1).reshape(2, needed * length, columns)
    far_full = jnp.concatenate([lower_flat, pairs[2], upper_flat], axis=1)
    extended = (first_ext, middle_ext, far_full)
    outputs = []
    log_sums = []
    for group_idx in range(3):
        group_out, log_sum = banded(
            query_list[group_idx],
            extended[group_idx][0],
            extended[group_idx][1],
            group_dilations[group_idx],
            offset_pos,
            seq_len,
        )
        outputs.append(group_out)
        log_sums.append(log_sum)
    merge_w = jax.nn.softmax(jnp.stack(log_sums, axis=0), axis=0)
    heads = columns // HEAD_DIM
    stacked = jnp.stack(outputs, axis=0).reshape(3, length, heads, HEAD_DIM)
    merged = (
        jnp.sum(merge_w[..., None] * stacked, axis=0).reshape(length, columns).astype(jnp.bfloat16)
    )
    mixed = jnp.dot(collect(merged, "tp", 1), out_weight, preferred_element_type=jnp.float32)
    return mixed.astype(jnp.bfloat16)


def solution(mesh):
    placed = (
        P("sp", None),
        P(None, None, "tp"),
        P(None, None, "tp"),
        P(None, None, "tp"),
        P(None, "tp"),
    )
    return jax.shard_map(
        per_device, mesh=mesh, in_specs=placed, out_specs=P("sp", "tp"), check_vma=False
    )
```

profile of v0, /device:TPU:568, one launch (start us, length us, event | category | flops | bytes accessed | tf_op | source)
XLA Modules:
  0.0 123.3 jit_solution(3061904734005105868)
XLA Ops:
  0.0 1.5 %slice_bitcast_fusion.4 = (bf16[128,2048]{0,1:T(8,128)(2,1)S(1)}, bf16[128,2048]{0,1:T(8,128)(2,1)S(1)}, bf16[128,2048]{0,1:T(8,128)(2,1)S(1)}) fusion(bf16[3,2048,128]{2,1,0:T(8,128)(2,1)} %param.7), kind=kLoop, calls=%fused_computation.46 | loop fusion | bytes 3145728 | tf_op jit(solution)/shard_map/dot_general | solution.py:121
  2.0 0.5 fusion.8
  2.8 1.6 %convolution_convert_fusion.1 = bf16[256,128]{1,0:T(8,128)(2,1)S(1)} fusion(bf16[256,2048]{1,0:T(8,128)(2,1)S(1)} %copy-done, bf16[3,2048,128]{2,1,0:T(8,128)(2,1)} %param.8), kind=kOutput, calls=%fused_computation.10 | convolution fusion | flops 134250496 | bytes 1638400 | tf_op jit(solution)/shard_map/dot_general | solution.py:123
  4.3 0.7 pad_maximum_fusion.2
  5.0 3.2 %collective-permute-start.6 = (bf16[2,256,128]{2,1,0:T(8,128)(2,1)}, bf16[2,256,128]{2,1,0:T(8,128)(2,1)}, u32[]{:S(2)}, u32[]{:S(2)}) collective-permute-start(bf16[2,256,128]{2,1,0:T(8,128)(2,1)} %pad_maximum_fusion.2), channel_id=1, source_target_pairs={{8,0},{16,8},{24,16},{32,24},{40,32},{48,40},{56,48},{64,56},{72,6... | collective-permute-start | bytes 393224 | tf_op jit(solution)/shard_map/ppermute | solution.py:30
  8.3 4.0 %collective-permute-start.7 = (bf16[2,256,128]{2,1,0:T(8,128)(2,1)}, bf16[2,256,128]{2,1,0:T(8,128)(2,1)}, u32[]{:S(2)}, u32[]{:S(2)}) collective-permute-start(bf16[2,256,128]{2,1,0:T(8,128)(2,1)} %pad_maximum_fusion.2), channel_id=1, source_target_pairs={{16,0},{24,8},{32,16},{40,24},{48,32},{56,40},{64,48},{72,56},{80,... | collective-permute-start | bytes 393224 | tf_op jit(solution)/shard_map/ppermute | solution.py:30
  12.3 2.1 %collective-permute-start.8 = (bf16[2,256,128]{2,1,0:T(8,128)(2,1)}, bf16[2,256,128]{2,1,0:T(8,128)(2,1)}, u32[]{:S(2)}, u32[]{:S(2)}) collective-permute-start(bf16[2,256,128]{2,1,0:T(8,128)(2,1)} %pad_maximum_fusion.2), channel_id=1, source_target_pairs={{24,0},{32,8},{40,16},{48,24},{56,32},{64,40},{72,48},{80,56},{88,... | collective-permute-start | bytes 393224 | tf_op jit(solution)/shard_map/ppermute | solution.py:30
  14.5 8.0 %collective-permute-start.9 = (bf16[2,256,128]{2,1,0:T(8,128)(2,1)}, bf16[2,256,128]{2,1,0:T(8,128)(2,1)}, u32[]{:S(2)}, u32[]{:S(2)}) collective-permute-start(bf16[2,256,128]{2,1,0:T(8,128)(2,1)} %pad_maximum_fusion.2), channel_id=1, source_target_pairs={{32,0},{40,8},{48,16},{56,24},{64,32},{72,40},{80,48},{88,56},{96,... | collective-permute-start | bytes 393224 | tf_op jit(solution)/shard_map/ppermute | solution.py:30
  22.5 4.7 %collective-permute-start.2 = (bf16[2,256,128]{2,1,0:T(8,128)(2,1)}, bf16[2,256,128]{2,1,0:T(8,128)(2,1)}, u32[]{:S(2)}, u32[]{:S(2)}) collective-permute-start(bf16[2,256,128]{2,1,0:T(8,128)(2,1)} %pad_maximum_fusion.2), channel_id=1, source_target_pairs={{0,8},{8,16},{16,24},{24,32},{32,40},{40,48},{48,56},{56,64},{64,7... | collective-permute-start | bytes 393224 | tf_op jit(solution)/shard_map/ppermute | solution.py:30
  27.2 0.4 convolution_convert_fusion.2
  27.7 0.4 convolution_convert_fusion.3
  28.1 0.5 iota_multiply_fusion
  28.7 0.6 fusion.81
  29.5 0.5 fusion.14
  30.2 0.5 fusion.16
  30.7 0.9 copy-done.1
  32.0 0.5 fusion.10
  32.7 0.5 fusion.12
  33.4 0.5 fusion.18
  34.2 0.7 broadcast_and_fusion.2
  35.0 0.7 broadcast_and_fusion
  36.4 0.8 copy.105
  37.2 0.8 copy.102
  38.0 0.7 copy.97
  38.6 0.8 convert_element_type.135
  40.0 0.8 copy.131
  40.8 0.8 copy.135
  41.9 0.8 pad_maximum_fusion.1
  42.7 2.0 %collective-permute-start.3 = (bf16[2,256,128]{2,1,0:T(8,128)(2,1)}, bf16[2,256,128]{2,1,0:T(8,128)(2,1)S(1)}, u32[]{:S(2)}, u32[]{:S(2)}) collective-permute-start(bf16[2,256,128]{2,1,0:T(8,128)(2,1)} %pad_maximum_fusion.2), channel_id=1, source_target_pairs={{0,16},{8,24},{16,32},{24,40},{32,48},{40,56},{48,64},{56,72},{64,... | collective-permute-start | bytes 393224 | tf_op jit(solution)/shard_map/ppermute | solution.py:30
  44.7 4.1 %collective-permute-start.4 = (bf16[2,256,128]{2,1,0:T(8,128)(2,1)}, bf16[2,256,128]{2,1,0:T(8,128)(2,1)S(1)}, u32[]{:S(2)}, u32[]{:S(2)}) collective-permute-start(bf16[2,256,128]{2,1,0:T(8,128)(2,1)} %pad_maximum_fusion.2), channel_id=1, source_target_pairs={{0,24},{8,32},{16,40},{24,48},{32,56},{40,64},{48,72},{56,80},{64,... | collective-permute-start | bytes 393224 | tf_op jit(solution)/shard_map/ppermute | solution.py:30
  48.8 5.9 %collective-permute-start.5 = (bf16[2,256,128]{2,1,0:T(8,128)(2,1)}, bf16[2,256,128]{2,1,0:T(8,128)(2,1)S(1)}, u32[]{:S(2)}, u32[]{:S(2)}) collective-permute-start(bf16[2,256,128]{2,1,0:T(8,128)(2,1)} %pad_maximum_fusion.2), channel_id=1, source_target_pairs={{0,32},{8,40},{16,48},{24,56},{32,64},{40,72},{48,80},{56,88},{64,... | collective-permute-start | bytes 393224 | tf_op jit(solution)/shard_map/ppermute | solution.py:30
  54.8 1.9 %collective-permute-start = (bf16[4,256,128]{2,1,0:T(8,128)(2,1)}, bf16[4,256,128]{2,1,0:T(8,128)(2,1)}, u32[]{:S(2)}, u32[]{:S(2)}) collective-permute-start(bf16[4,256,128]{2,1,0:T(8,128)(2,1)} %pad_maximum_fusion.1), channel_id=1, source_target_pairs={{0,8},{8,16},{16,24},{24,32},{32,40},{40,48},{48,56},{56,64},{64,7... | collective-permute-start | bytes 786440 | tf_op jit(solution)/shard_map/ppermute | solution.py:19
  56.7 1.2 maximum_bitcast_fusion
  58.0 1.0 copy.121
  59.2 1.0 copy.122
  60.4 1.0 copy.123
  61.5 1.0 copy.124
  62.6 4.1 %collective-permute-start.1 = (bf16[4,256,128]{2,1,0:T(8,128)(2,1)}, bf16[4,256,128]{2,1,0:T(8,128)(2,1)}, u32[]{:S(2)}, u32[]{:S(2)}) collective-permute-start(bf16[4,256,128]{2,1,0:T(8,128)(2,1)} %pad_maximum_fusion.1), channel_id=1, source_target_pairs={{8,0},{16,8},{24,16},{32,24},{40,32},{48,40},{56,48},{64,56},{72,6... | collective-permute-start | bytes 786440 | tf_op jit(solution)/shard_map/ppermute | solution.py:22
  66.7 6.0 %collective-permute-done.3 = bf16[2,256,128]{2,1,0:T(8,128)(2,1)S(1)} collective-permute-done((bf16[2,256,128]{2,1,0:T(8,128)(2,1)}, bf16[2,256,128]{2,1,0:T(8,128)(2,1)S(1)}, u32[]{:S(2)}, u32[]{:S(2)}) %collective-permute-start.3) | collective-permute-done | bytes 131104 | tf_op jit(solution)/shard_map/ppermute | solution.py:30
  72.7 1.0 pad_maximum_fusion
  73.9 1.0 copy.116
  75.0 1.0 copy.117
  76.2 1.0 copy.118
  77.3 1.1 copy.119
  78.5 1.0 copy.143
  79.7 1.0 copy.144
  80.8 1.0 copy.145
  82.0 1.1 copy.146
  83.1 1.0 copy.138
  84.3 1.0 copy.139
  85.4 1.0 copy.140
  86.5 1.0 copy.141
  87.6 5.2 %concatenate.82 = bf16[1,144,16,2,64]{1,4,3,2,0:T(8,128)(2,1)S(1)} concatenate(bf16[1,16,16,2,64]{1,4,3,2,0:T(8,128)(2,1)} %copy.116, bf16[1,16,16,2,64]{1,4,3,2,0:T(8,128)(2,1)} %copy.117, bf16[1,16,16,2,64]{1,4,3,2,0:T(8,128)(2,1)} %copy.118, bf16[1,16,16,2,64]{1,4,3,2,0:T(8,128)(2,1)} %copy.119, bf16[1,16,16,2,64]{1,4,3,2,0:T(8,128)(2,1)S(1)} %copy.120, ...), dimensions={1} | concatenate | bytes 1179648 | tf_op jit(solution)/shard_map/concatenate | solution.py:75
  92.7 1.2 fusion.104
  94.2 5.2 %concatenate.85 = bf16[1,144,16,2,64]{1,4,3,2,0:T(8,128)(2,1)S(1)} concatenate(bf16[1,16,16,2,64]{1,4,3,2,0:T(8,128)(2,1)} %copy.138, bf16[1,16,16,2,64]{1,4,3,2,0:T(8,128)(2,1)} %copy.139, bf16[1,16,16,2,64]{1,4,3,2,0:T(8,128)(2,1)} %copy.140, bf16[1,16,16,2,64]{1,4,3,2,0:T(8,128)(2,1)} %copy.141, bf16[1,16,16,2,64]{1,4,3,2,0:T(8,128)(2,1)S(1)} %copy.142, ...), dimensions={1} | concatenate | bytes 1179648 | tf_op jit(solution)/shard_map/concatenate | solution.py:78
  99.4 0.4 fusion.5
  100.4 0.9 pad_maximum_fusion.7
  101.6 0.9 pad_maximum_fusion.3
  102.9 0.4 fusion.105
  104.4 0.4 fusion.106
  105.8 0.3 fusion.3
  107.1 0.3 fusion.4
  107.8 14.4 %all_to_all.5 = bf16[8,256,128]{1,2,0:T(8,128)(2,1)S(1)} all-to-all(bf16[8,256,128]{1,2,0:T(8,128)(2,1)S(1)} %broadcast_in_dim.29), channel_id=1, replica_groups=mesh['sp'=96,'tp'=8] {'tp'}, dimensions={0} | all-to-all | bytes 1048576 | tf_op jit(solution)/shard_map/all_to_all | solution.py:41
  122.3 1.0 convolution_convert_fusion
  (150 shorter events, 10.0 us)
Async XLA Ops:
  0.0 2.0 %copy-start = (bf16[256,2048]{1,0:T(8,128)(2,1)S(1)}, bf16[256,2048]{1,0:T(8,128)(2,1)}, u32[]{:S(2)}) copy-start(bf16[256,2048]{1,0:T(8,128)(2,1)} %param.5) | copy-start | bytes 3145732
  1.8 0.8 copy-start.2
  1.8 0.8 copy-start.4
  2.6 25.1 %copy-start.6 = (bf16[256,2,64]{0,2,1:T(8,128)(2,1)}, bf16[256,2,64]{0,2,1:T(8,128)(2,1)S(1)}, u32[]{:S(2)}) copy-start(bf16[256,2,64]{0,2,1:T(8,128)(2,1)S(1)} %fusion.66) | copy-start | bytes 196612
  2.7 24.5 %copy-start.20 = (bf16[3,2048,128]{2,1,0:T(8,128)(2,1)S(1)}, bf16[3,2048,128]{2,1,0:T(8,128)(2,1)}, u32[]{:S(2)}) copy-start(bf16[3,2048,128]{2,1,0:T(8,128)(2,1)} %param.8) | copy-start | bytes 4718596
  4.3 23.8 %copy-start.8 = (bf16[256,128]{1,0:T(8,128)(2,1)}, bf16[256,128]{1,0:T(8,128)(2,1)S(1)}, u32[]{:S(2)}) copy-start(bf16[256,128]{1,0:T(8,128)(2,1)S(1)} %convolution_convert_fusion.1) | copy-start | bytes 196612
  5.0 37.6 %collective-permute-start.6 = (bf16[2,256,128]{2,1,0:T(8,128)(2,1)}, bf16[2,256,128]{2,1,0:T(8,128)(2,1)}, u32[]{:S(2)}, u32[]{:S(2)}) collective-permute-start(bf16[2,256,128]{2,1,0:T(8,128)(2,1)} %pad_maximum_fusion.2), channel_id=1, source_target_pairs={{8,0},{16,8},{24,16},{32,24},{40,32},{48,40},{56,48},{64,56},{72,6... | collective-permute-start | bytes 393224 | tf_op jit(solution)/shard_map/ppermute | solution.py:30
  8.3 36.4 %collective-permute-start.7 = (bf16[2,256,128]{2,1,0:T(8,128)(2,1)}, bf16[2,256,128]{2,1,0:T(8,128)(2,1)}, u32[]{:S(2)}, u32[]{:S(2)}) collective-permute-start(bf16[2,256,128]{2,1,0:T(8,128)(2,1)} %pad_maximum_fusion.2), channel_id=1, source_target_pairs={{16,0},{24,8},{32,16},{40,24},{48,32},{56,40},{64,48},{72,56},{80,... | collective-permute-start | bytes 393224 | tf_op jit(solution)/shard_map/ppermute | solution.py:30
  12.3 36.5 %collective-permute-start.8 = (bf16[2,256,128]{2,1,0:T(8,128)(2,1)}, bf16[2,256,128]{2,1,0:T(8,128)(2,1)}, u32[]{:S(2)}, u32[]{:S(2)}) collective-permute-start(bf16[2,256,128]{2,1,0:T(8,128)(2,1)} %pad_maximum_fusion.2), channel_id=1, source_target_pairs={{24,0},{32,8},{40,16},{48,24},{56,32},{64,40},{72,48},{80,56},{88,... | collective-permute-start | bytes 393224 | tf_op jit(solution)/shard_map/ppermute | solution.py:30
  14.5 40.3 %collective-permute-start.9 = (bf16[2,256,128]{2,1,0:T(8,128)(2,1)}, bf16[2,256,128]{2,1,0:T(8,128)(2,1)}, u32[]{:S(2)}, u32[]{:S(2)}) collective-permute-start(bf16[2,256,128]{2,1,0:T(8,128)(2,1)} %pad_maximum_fusion.2), channel_id=1, source_target_pairs={{32,0},{40,8},{48,16},{56,24},{64,32},{72,40},{80,48},{88,56},{96,... | collective-permute-start | bytes 393224 | tf_op jit(solution)/shard_map/ppermute | solution.py:30
  22.5 40.0 %collective-permute-start.2 = (bf16[2,256,128]{2,1,0:T(8,128)(2,1)}, bf16[2,256,128]{2,1,0:T(8,128)(2,1)}, u32[]{:S(2)}, u32[]{:S(2)}) collective-permute-start(bf16[2,256,128]{2,1,0:T(8,128)(2,1)} %pad_maximum_fusion.2), channel_id=1, source_target_pairs={{0,8},{8,16},{16,24},{24,32},{32,40},{40,48},{48,56},{56,64},{64,7... | collective-permute-start | bytes 393224 | tf_op jit(solution)/shard_map/ppermute | solution.py:30
  30.2 1.4 %copy-start.1 = (bf16[3,2048,128]{2,1,0:T(8,128)(2,1)S(1)}, bf16[3,2048,128]{2,1,0:T(8,128)(2,1)}, u32[]{:S(2)}) copy-start(bf16[3,2048,128]{2,1,0:T(8,128)(2,1)} %param.6) | copy-start | bytes 4718596
  33.4 0.7 copy-start.19
  33.4 1.5 %copy-start.3 = (f32[256,64]{0,1:T(8,128)S(1)}, f32[256,64]{0,1:T(8,128)}, u32[]{:S(2)}) copy-start(f32[256,64]{0,1:T(8,128)} %copy-done.2) | copy-start | bytes 196612
  33.4 1.5 %copy-start.5 = (f32[256,64]{0,1:T(8,128)S(1)}, f32[256,64]{0,1:T(8,128)}, u32[]{:S(2)}) copy-start(f32[256,64]{0,1:T(8,128)} %copy-done.4) | copy-start | bytes 196612
  33.9 1.1 copy-start.18
  33.9 1.7 %copy-start.7 = (bf16[256,2,64]{0,2,1:T(8,128)(2,1)S(1)}, bf16[256,2,64]{0,2,1:T(8,128)(2,1)}, u32[]{:S(2)}) copy-start(bf16[256,2,64]{0,2,1:T(8,128)(2,1)} %copy-done.6) | copy-start | bytes 196612
  34.0 1.8 %copy-start.9 = (bf16[256,128]{1,0:T(8,128)(2,1)S(1)}, bf16[256,128]{1,0:T(8,128)(2,1)}, u32[]{:S(2)}) copy-start(bf16[256,128]{1,0:T(8,128)(2,1)} %copy-done.8) | copy-start | bytes 196612
  42.7 30.0 %collective-permute-start.3 = (bf16[2,256,128]{2,1,0:T(8,128)(2,1)}, bf16[2,256,128]{2,1,0:T(8,128)(2,1)S(1)}, u32[]{:S(2)}, u32[]{:S(2)}) collective-permute-start(bf16[2,256,128]{2,1,0:T(8,128)(2,1)} %pad_maximum_fusion.2), channel_id=1, source_target_pairs={{0,16},{8,24},{16,32},{24,40},{32,48},{40,56},{48,64},{56,72},{64,... | collective-permute-start | bytes 393224 | tf_op jit(solution)/shard_map/ppermute | solution.py:30
  44.7 27.9 %collective-permute-start.4 = (bf16[2,256,128]{2,1,0:T(8,128)(2,1)}, bf16[2,256,128]{2,1,0:T(8,128)(2,1)S(1)}, u32[]{:S(2)}, u32[]{:S(2)}) collective-permute-start(bf16[2,256,128]{2,1,0:T(8,128)(2,1)} %pad_maximum_fusion.2), channel_id=1, source_target_pairs={{0,24},{8,32},{16,40},{24,48},{32,56},{40,64},{48,72},{56,80},{64,... | collective-permute-start | bytes 393224 | tf_op jit(solution)/shard_map/ppermute | solution.py:30
  48.8 23.9 %collective-permute-start.5 = (bf16[2,256,128]{2,1,0:T(8,128)(2,1)}, bf16[2,256,128]{2,1,0:T(8,128)(2,1)S(1)}, u32[]{:S(2)}, u32[]{:S(2)}) collective-permute-start(bf16[2,256,128]{2,1,0:T(8,128)(2,1)} %pad_maximum_fusion.2), channel_id=1, source_target_pairs={{0,32},{8,40},{16,48},{24,56},{32,64},{40,72},{48,80},{56,88},{64,... | collective-permute-start | bytes 393224 | tf_op jit(solution)/shard_map/ppermute | solution.py:30
  54.8 45.7 %collective-permute-start = (bf16[4,256,128]{2,1,0:T(8,128)(2,1)}, bf16[4,256,128]{2,1,0:T(8,128)(2,1)}, u32[]{:S(2)}, u32[]{:S(2)}) collective-permute-start(bf16[4,256,128]{2,1,0:T(8,128)(2,1)} %pad_maximum_fusion.1), channel_id=1, source_target_pairs={{0,8},{8,16},{16,24},{24,32},{32,40},{40,48},{48,56},{56,64},{64,7... | collective-permute-start | bytes 786440 | tf_op jit(solution)/shard_map/ppermute | solution.py:19
  62.6 39.1 %collective-permute-start.1 = (bf16[4,256,128]{2,1,0:T(8,128)(2,1)}, bf16[4,256,128]{2,1,0:T(8,128)(2,1)}, u32[]{:S(2)}, u32[]{:S(2)}) collective-permute-start(bf16[4,256,128]{2,1,0:T(8,128)(2,1)} %pad_maximum_fusion.1), channel_id=1, source_target_pairs={{8,0},{16,8},{24,16},{32,24},{40,32},{48,40},{56,48},{64,56},{72,6... | collective-permute-start | bytes 786440 | tf_op jit(solution)/shard_map/ppermute | solution.py:22
  100.3 2.6 %copy-start.11 = (bf16[256,2,64]{2,0,1:T(8,128)(2,1)S(1)}, bf16[256,2,64]{2,0,1:T(8,128)(2,1)}, u32[]{:S(2)}) copy-start(bf16[256,2,64]{2,0,1:T(8,128)(2,1)} %copy.102) | copy-start | bytes 196612
  100.3 2.6 %copy-start.15 = (bf16[1,64,4,2,64]{1,4,3,2,0:T(8,128)(2,1)S(1)}, bf16[1,64,4,2,64]{1,4,3,2,0:T(8,128)(2,1)}, u32[]{:S(2)}) copy-start(bf16[1,64,4,2,64]{1,4,3,2,0:T(8,128)(2,1)} %copy.105) | copy-start | bytes 196612
  100.3 2.6 %copy-start.17 = (pred[4,64,192]{2,1,0:T(8,128)(4,1)S(1)}, pred[4,64,192]{2,1,0:T(8,128)(4,1)}, u32[]{:S(2)}) copy-start(pred[4,64,192]{2,1,0:T(8,128)(4,1)} %get-tuple-element.57) | copy-start | bytes 147460
  102.8 1.6 %copy-start.10 = (bf16[4,64,2,64]{1,0,3,2:T(4,128)(2,1)S(1)}, bf16[4,64,2,64]{1,0,3,2:T(4,128)(2,1)}, u32[]{:S(2)}) copy-start(bf16[4,64,2,64]{1,0,3,2:T(4,128)(2,1)} %convert_element_type.135) | copy-start | bytes 196612
  102.8 1.6 %copy-start.14 = (bf16[4,64,1,2,64]{1,4,3,0,2:T(8,128)(2,1)S(1)}, bf16[4,64,1,2,64]{1,4,3,0,2:T(8,128)(2,1)}, u32[]{:S(2)}) copy-start(bf16[4,64,1,2,64]{1,4,3,0,2:T(8,128)(2,1)} %copy.97) | copy-start | bytes 196612
  102.8 1.6 %copy-start.16 = (pred[4,64,192]{2,1,0:T(8,128)(4,1)S(1)}, pred[4,64,192]{2,1,0:T(8,128)(4,1)}, u32[]{:S(2)}) copy-start(pred[4,64,192]{2,1,0:T(8,128)(4,1)} %get-tuple-element.56) | copy-start | bytes 147460
  104.3 1.6 %copy-start.13 = (bf16[4,64,1,2,64]{1,4,3,0,2:T(8,128)(2,1)S(1)}, bf16[4,64,1,2,64]{1,4,3,0,2:T(8,128)(2,1)}, u32[]{:S(2)}) copy-start(bf16[4,64,1,2,64]{1,4,3,0,2:T(8,128)(2,1)} %copy.131) | copy-start | bytes 196612
  105.8 1.2 %copy-start.12 = (bf16[1,64,4,2,64]{1,4,3,2,0:T(8,128)(2,1)S(1)}, bf16[1,64,4,2,64]{1,4,3,2,0:T(8,128)(2,1)}, u32[]{:S(2)}) copy-start(bf16[1,64,4,2,64]{1,4,3,2,0:T(8,128)(2,1)} %copy.135) | copy-start | bytes 196612
  107.4 14.9 %copy-start.21 = (bf16[1024,256]{1,0:T(8,128)(2,1)S(1)}, bf16[1024,256]{1,0:T(8,128)(2,1)}, u32[]{:S(2)}) copy-start(bf16[1024,256]{1,0:T(8,128)(2,1)} %param.9) | copy-start | bytes 1572868
where the time goes:
time: 124 us; the launch traced here: 123 us
  local copies, waits for them, and re-layouts  42.5 us (34%)
  starting transfers between devices  40.2 us (32%)
  blocking collectives  14.4 us (12%)
  matrix products  9.46 us (8%)
  other arithmetic  9.45 us (8%)
  waiting for transfers between devices  6.02 us (5%)
    ppermute x8, starting transfers between devices, shifted(): return lax.ppermute(block, axis, route)  34.2 us
    all_to_all x1, blocking collectives, copy_for_each(): lax.all_to_all(jnp.broadcast_to(value[None], (size, *value.shape)), axis,...  14.4 us
    slice x30, local copies, waits for them, and re-layouts, banded(): value_blocks[shift_idx:shift_idx + blocks]  12.2 us
    slice x26, local copies, waits for them, and re-layouts, banded(): key_blocks[shift_idx:shift_idx + blocks]  10.2 us
    ppermute x8, waiting for transfers between devices, shifted(): return lax.ppermute(block, axis, route)  6.02 us
    concatenate x1, local copies, waits for them, and re-layouts, banded(): jnp.concatenate([value_blocks[shift_idx:shift_idx + blocks] for shift_idx...  5.17 us
    concatenate x1, local copies, waits for them, and re-layouts, banded(): jnp.concatenate([key_blocks[shift_idx:shift_idx + blocks] for shift_idx i...  5.15 us
    ppermute x1, starting transfers between devices, with_halo(): lax.ppermute(lax.slice_in_dim(block, 0, width, axis=dim), axis, backward)  4.09 us
  transfers between devices with their start and end apart: 10, of which 1 were waited for; matrix products, arithmetic and copies ran while one was open for 40% of the time, Pallas kernels for 0%

commit v1 on v0

v1 whole, which is shorter than its diff:
```python
import functools

import jax
import jax.numpy as jnp
import numpy as np
from jax import lax
from jax.experimental import pallas as pl
from jax.experimental.pallas import tpu as pltpu
from jax.sharding import PartitionSpec as P

HEAD_DIM = 64
SIDE = 64
MIDDLE = 4
FAR = 16
LANES = 128
ROW = 8
BF = jnp.bfloat16
F32 = jnp.float32
SPLIT = 4


def rotary_tables(devices, length):
    lane = np.arange(LANES)
    inverse = 10000.0 ** (-2.0 * (lane % (HEAD_DIM // 2)) / HEAD_DIM)
    sign = np.where(lane % HEAD_DIM < HEAD_DIM // 2, -1.0, 1.0)
    base = np.arange(devices)[:, None] * length * inverse[None]
    step = np.arange(length)[:, None] * inverse[None]
    far = np.concatenate([np.cos(base), np.sin(base), sign * np.cos(base), sign * np.sin(base)], axis=1)
    near = np.stack([np.cos(step), np.sin(step)])
    return far.astype(np.float32), near.astype(np.float32)


def turn_tables(far_ref, near_ref):
    row = far_ref[pl.ds(lax.axis_index("sp"), 1), :]
    cos_base, sin_base = row[:, :LANES], row[:, LANES : 2 * LANES]
    scos_base, ssin_base = row[:, 2 * LANES : 3 * LANES], row[:, 3 * LANES :]
    cos_step, sin_step = near_ref[0], near_ref[1]
    return cos_base * cos_step - sin_base * sin_step, ssin_base * cos_step + scos_base * sin_step


def swap_halves(x):
    lane = lax.broadcasted_iota(jnp.int32, x.shape, 1)
    half = HEAD_DIM // 2
    return jnp.where(
        lane % HEAD_DIM < half, pltpu.roll(x, LANES - half, 1), pltpu.roll(x, half, 1)
    )


def rotate(x, tables):
    return x * tables[0] + swap_halves(x) * tables[1]


def store_by_class(x, scratch, out, dilation):
    scratch[...] = x
    n = x.shape[0] // dilation
    for c in range(dilation):
        out[pl.ds(c * n, n), :] = scratch[pl.ds(c, n, stride=dilation), :].astype(BF)


def far_kernel(tok, wk, wv, far, near, out, acc, scratch):
    step = pl.program_id(0)

    @pl.when(step == 0)
    def _():
        acc[...] = jnp.zeros_like(acc)

    x = tok[...]
    acc[0] += jnp.dot(x, wk[0], preferred_element_type=F32)
    acc[1] += jnp.dot(x, wv[0], preferred_element_type=F32)

    @pl.when(step == SPLIT - 1)
    def _():
        tables = turn_tables(far, near)
        store_by_class(rotate(acc[0], tables), scratch.at[0], out.at[0], FAR)
        store_by_class(acc[1], scratch.at[1], out.at[1], FAR)


def rest_kernel(tok, wq, wk, wv, far, near, q3, q12, kv1, up, down, acc, scratch):
    step = pl.program_id(0)

    @pl.when(step == 0)
    def _():
        acc[...] = jnp.zeros_like(acc)

    x = tok[...]
    for g in range(3):
        acc[g] += jnp.dot(x, wq[g], preferred_element_type=F32)
    for g in range(2):
        acc[3 + g] += jnp.dot(x, wk[g], preferred_element_type=F32)
        acc[5 + g] += jnp.dot(x, wv[g], preferred_element_type=F32)

    @pl.when(step == SPLIT - 1)
    def _():
        length = tok.shape[0]
        tables = turn_tables(far, near)
        store_by_class(rotate(acc[2], tables), scratch.at[0], q3, FAR)
        q12[0] = rotate(acc[0], tables).astype(BF)
        store_by_class(rotate(acc[1], tables), scratch.at[1], q12.at[1], MIDDLE)
        k1 = rotate(acc[3], tables).astype(BF)
        v1 = acc[5].astype(BF)
        for n, x1 in enumerate((k1, v1)):
            kv1[n] = x1
            up[n, pl.ds(length, SIDE), :] = x1[length - SIDE :]
            down[n, pl.ds(length, SIDE), :] = x1[:SIDE]
        middle = (rotate(acc[4], tables), acc[6])
        for n in range(2):
            scratch[2 + n] = middle[n]
            rows = length // MIDDLE
            for c in range(MIDDLE):
                part = scratch[2 + n, pl.ds(c, rows, stride=MIDDLE), :].astype(BF)
                up[n, pl.ds(c * rows, rows), :] = part
                down[n, pl.ds(c * rows, rows), :] = part


def attend(q, k, v, low, high):
    n, keys = q.shape[0], k.shape[0]
    lane = lax.broadcasted_iota(jnp.int32, (1, LANES), 1)
    first = (lane < HEAD_DIM).astype(F32).astype(BF)
    second = (lane >= HEAD_DIM).astype(F32).astype(BF)
    both = jnp.concatenate([q * first, q * second], axis=0)
    scores = lax.dot_general(both, k, (((1,), (1,)), ((), ())), preferred_element_type=F32)
    scores = scores * HEAD_DIM ** (-0.5)
    column = lax.broadcasted_iota(jnp.int32, (n, keys), 1)
    relative = column - lax.broadcasted_iota(jnp.int32, (n, keys), 0)
    allowed = (relative >= 0) & (relative <= 2 * SIDE) & (column >= low) & (column < high)
    outs, tops, sums = [], [], []
    for head in range(2):
        part = jnp.where(allowed, scores[head * n : (head + 1) * n], -1e30)
        top = jnp.max(part, axis=-1, keepdims=True)
        expo = jnp.exp(part - top)
        sums.append(jnp.sum(expo, axis=-1, keepdims=True))
        tops.append(top)
        outs.append(jnp.dot(expo.astype(BF), v, preferred_element_type=F32))
    is_first = lax.broadcasted_iota(jnp.int32, (n, LANES), 1) < HEAD_DIM
    denom = jnp.where(is_first, sums[0], sums[1])
    top = jnp.where(is_first, tops[0], tops[1])
    return jnp.where(is_first, outs[0], outs[1]) / denom, top + jnp.log(denom)


def merge(out_a, lse_a, out_b, lse_b):
    top = jnp.maximum(lse_a, lse_b)
    wa, wb = jnp.exp(lse_a - top), jnp.exp(lse_b - top)
    total = wa + wb
    return (wa * out_a + wb * out_b) / total, top + jnp.log(total)


def near_attention_kernel(devices, q12, kv1, up, low, high, out, lse, out2, lse2):
    length = kv1.shape[1]
    me = lax.axis_index("sp")
    rows = length // MIDDLE
    start = jnp.where(me == 0, SIDE, 0)
    for c in range(MIDDLE):
        at = pl.ds(c * rows, rows)
        k = jnp.concatenate([low[0, at, :], up[0, at, :], high[0, at, :]], axis=0)
        v = jnp.concatenate([low[1, at, :], up[1, at, :], high[1, at, :]], axis=0)
        o, l = attend(
            q12[1, at, :], k, v, start, jnp.where(me == devices - 1, 2 * rows, 3 * rows)
        )
        out2[pl.ds(c, rows, stride=MIDDLE), :] = o
        lse2[pl.ds(c, rows, stride=MIDDLE), :] = l
    block = 2 * SIDE
    for b in range(length // block):
        ks, vs = [], []
        for n, xs in enumerate((ks, vs)):
            if b == 0:
                xs.append(low[n, pl.ds(length, SIDE), :])
            first = max(b * block - SIDE, 0)
            last = min((b + 1) * block + SIDE, length)
            xs.append(kv1[n, pl.ds(first, last - first), :])
            if b == length // block - 1:
                xs.append(high[n, pl.ds(length, SIDE), :])
        at = pl.ds(b * block, block)
        o, l = attend(
            q12[0, at, :],
            jnp.concatenate(ks, axis=0),
            jnp.concatenate(vs, axis=0),
            start if b == 0 else 0,
            jnp.where(me == devices - 1, block + SIDE, 2 * block)
            if b == length // block - 1
            else 2 * block,
        )
        out[at, :], lse[at, :] = merge(o, l, out2[at, :], lse2[at, :])


def far_attention_kernel(rows_of_devices, parts, out):
    z = lax.axis_index("sp") // ROW
    low = jnp.where(z == 0, SIDE, 0)
    size = parts.shape[1] // 5
    run = size // 2
    half = ROW // 2
    queries = ROW * run
    high = jnp.where(z == rows_of_devices - 1, queries + SIDE, queries + 2 * SIDE)
    lane = lax.broadcasted_iota(jnp.int32, (queries, LANES), 1)
    for e in range(2):
        piece = lambda a, y: parts[y, pl.ds(a * size + e * run, run), :]
        q = jnp.concatenate([piece(0, y) for y in range(ROW)], axis=0)
        kv = [
            jnp.concatenate(
                [piece(a + 2, y) for y in range(half, ROW)]
                + [piece(a, y) for y in range(ROW)]
                + [piece(a + 2, y) for y in range(half)],
                axis=0,
            )
            for a in (1, 2)
        ]
        o, l = attend(q, kv[0], kv[1], low, high)
        coarse = l.astype(BF).astype(F32)
        l = jnp.where(lane % HEAD_DIM < HEAD_DIM // 2, coarse, l - coarse).astype(BF)
        o = o.astype(BF)
        for y in range(ROW):
            out[y, pl.ds(e * run, run), :] = o[y * run : (y + 1) * run]
            out[y, pl.ds(size + e * run, run), :] = l[y * run : (y + 1) * run]


def merge_kernel(parts, out12, lse12, merged, out3, lse3):
    size = parts.shape[1] // 2
    run = size // 2
    for c in range(FAR):
        y, e = c // 2, c % 2
        at = pl.ds(c, run, stride=FAR)
        out3[at, :] = parts[y, pl.ds(e * run, run), :].astype(F32)
        lse3[at, :] = parts[y, pl.ds(size + e * run, run), :].astype(F32)
    l = lse3[...]
    o, _ = merge(out12[...], lse12[...], out3[...], l + swap_halves(l))
    merged[...] = o.astype(BF)


def vmem(shape):
    return jax.ShapeDtypeStruct(shape, BF)


def whole():
    return pl.BlockSpec(memory_space=pltpu.VMEM)


def cost(flops, size):
    return pl.CostEstimate(flops=flops, bytes_accessed=size, transcendentals=0)


def per_device(devices, tokens, query_weight, key_weight, value_weight, out_weight):
    length, width = tokens.shape
    columns = key_weight.shape[2]
    far, near = rotary_tables(devices, length)
    chunk = width // SPLIT
    fixed = [
        pl.BlockSpec(far.shape, lambda k: (0, 0)),
        pl.BlockSpec(near.shape, lambda k: (0, 0, 0)),
    ]
    token_spec = pl.BlockSpec((length, chunk), lambda k: (0, k))
    one = pl.BlockSpec((1, chunk, columns), lambda k: (2, k, 0))
    kv3 = pl.pallas_call(
        far_kernel,
        grid=(SPLIT,),
        in_specs=[token_spec, one, one] + fixed,
        out_specs=pl.BlockSpec((2, length, columns), lambda k: (0, 0, 0)),
        out_shape=vmem((2, length, columns)),
        scratch_shapes=[
            pltpu.VMEM((2, length, columns), F32),
            pltpu.VMEM((2, length, columns), F32),
        ],
        cost_estimate=cost(4 * length * width * columns, 2 << 20),
        name="far_keys_values",
    )(tokens, key_weight, value_weight, far, near)

    half = ROW // 2
    route = []
    for s in range(devices):
        target = s + ROW if s % ROW >= half else s - ROW
        if 0 <= target < devices:
            route.append((s, target))
    halo3 = lax.ppermute(kv3, "sp", route)

    two = pl.BlockSpec((2, chunk, columns), lambda k: (0, k, 0))
    edge = length + SIDE
    shapes = [
        (length, columns),
        (2, length, columns),
        (2, length, columns),
        (2, edge, columns),
        (2, edge, columns),
    ]
    q3, q12, kv1, up, down = pl.pallas_call(
        rest_kernel,
        grid=(SPLIT,),
        in_specs=[token_spec, pl.BlockSpec((3, chunk, columns), lambda k: (0, k, 0)), two, two]
        + fixed,
        out_specs=[
            pl.BlockSpec(s, functools.partial(lambda n, k: (0,) * n, len(s))) for s in shapes
        ],
        out_shape=[vmem(s) for s in shapes],
        scratch_shapes=[
            pltpu.VMEM((7, length, columns), F32),
            pltpu.VMEM((4, length, columns), F32),
        ],
        cost_estimate=cost(14 * length * width * columns, 5 << 20),
        name="projections",
    )(tokens, query_weight, key_weight, value_weight, far, near)

    low = lax.ppermute(up, "sp", [(s, s + 1) for s in range(devices - 1)])
    high = lax.ppermute(down, "sp", [(s + 1, s) for s in range(devices - 1)])

    size = length // ROW
    packed = jnp.concatenate([q3[None], kv3, halo3], axis=0).reshape(5, ROW, size, columns)
    packed = jnp.swapaxes(packed, 0, 1).reshape(ROW, 5 * size, columns)
    groups = [[z * ROW + y for y in range(ROW)] for z in range(devices // ROW)]
    parts = lax.all_to_all(packed, "sp", 0, 0, axis_index_groups=groups, tiled=True)

    back = pl.pallas_call(
        functools.partial(far_attention_kernel, devices // ROW),
        in_specs=[whole()],
        out_specs=whole(),
        out_shape=vmem((ROW, 2 * size, columns)),
        cost_estimate=cost(1 << 27, 1 << 19),
        name="far_attention",
    )(parts)
    parts3 = lax.all_to_all(back, "sp", 0, 0, axis_index_groups=groups, tiled=True)

    flat = jax.ShapeDtypeStruct((length, columns), F32)
    out12, lse12 = pl.pallas_call(
        functools.partial(near_attention_kernel, devices),
        in_specs=[whole()] * 5,
        out_specs=[whole()] * 2,
        out_shape=[flat, flat],
        scratch_shapes=[pltpu.VMEM((length, columns), F32)] * 2,
        cost_estimate=cost(1 << 28, 1 << 20),
        name="near_attention",
    )(q12, kv1, up, low, high)

    merged = pl.pallas_call(
        merge_kernel,
        in_specs=[whole()] * 3,
        out_specs=whole(),
        out_shape=vmem((length, columns)),
        scratch_shapes=[pltpu.VMEM((length, columns), F32)] * 2,
        cost_estimate=cost(1 << 20, 1 << 19),
        name="merge",
    )(parts3, out12, lse12)

    gathered = lax.all_gather(merged, "tp", axis=0, tiled=False)
    gathered = jnp.swapaxes(gathered, 0, 1).reshape(length, -1)
    mixed = jnp.dot(gathered, out_weight, preferred_element_type=F32)
    return mixed.astype(BF)


def solution(mesh):
    weights = P(None, None, "tp")
    return jax.shard_map(
        functools.partial(per_device, mesh.shape["sp"]),
        mesh=mesh,
        in_specs=(P("sp", None), weights, weights, weights, P(None, "tp")),
        out_specs=P("sp", "tp"),
        check_vma=False,
    )
```

time: 124 us -> 78.5 us (0.63)
  the two profiles are of different devices: /device:TPU:568 before, /device:TPU:249 now
where the time goes in v1:
time: 78.5 us; the launch traced here: 78 us
  blocking collectives  32.2 us (41%)
  starting transfers between devices  17.5 us (22%)
  Pallas kernels  17.3 us (22%)
  waiting for transfers between devices  7.46 us (10%)
  local copies, waits for them, and re-layouts  1.55 us (2%)
  matrix products  1 us (1%)
  other arithmetic  0.91 us (1%)
    all_gather x1, blocking collectives, per_device(): gathered = lax.all_gather(merged, 'tp', axis=0, tiled=False)  17.6 us
    all_to_all x1, blocking collectives, per_device(): lax.all_to_all(packed, 'sp', 0, 0, axis_index_groups=groups, tiled=True)  14.6 us
    all_to_all x1, starting transfers between devices, per_device(): lax.all_to_all(back, 'sp', 0, 0, axis_index_groups=groups, tiled=True)  6.44 us
    pallas_call x1, Pallas kernels, per_device(): pl.pallas_call(rest_kernel, grid=(SPLIT,), in_specs=[token_spec, pl.Block...  6.04 us
    ppermute x1, waiting for transfers between devices, per_device(): high = lax.ppermute(down, 'sp', [(s + 1, s) for s in range(devices - 1)])  5.45 us
    ppermute x1, starting transfers between devices, per_device(): halo3 = lax.ppermute(kv3, 'sp', route)  5.33 us
    pallas_call x1, Pallas kernels, per_device(): pl.pallas_call(far_kernel, grid=(SPLIT,), in_specs=[token_spec, one, one]...  4.16 us
    ppermute x1, starting transfers between devices, per_device(): low = lax.ppermute(up, 'sp', [(s, s + 1) for s in range(devices - 1)])  3.79 us
  transfers between devices with their start and end apart: 4, of which 2 were waited for; matrix products, arithmetic and copies ran while one was open for 0% of the time, Pallas kernels for 11%

profile of v1, /device:TPU:249, one launch (start us, length us, event | category | flops | bytes accessed | tf_op | source)
XLA Modules:
  0.0 78.0 jit_solution(2557597752841040810)
XLA Ops:
  0.0 0.0 copy-start
  0.0 4.2 %far_keys_values.1 = bf16[2,256,128]{2,1,0:T(8,128)(2,1)} custom-call(bf16[256,2048]{1,0:T(8,128)(2,1)} %tok.3, bf16[3,2048,128]{2,1,0:T(8,128)(2,1)} %wk.3, bf16[3,2048,128]{2,1,0:T(8,128)(2,1)} %wv.3, f32[96,512]{1,0:T(8,128)} %constant.4.clone.far, f32[2,256,128]{2,1,0:T(8,128)} %constant.5.clone.near), custom_call_target="tpu_custom_call" | custom-call | flops 268435456 | bytes 2097152 | tf_op jit(solution)/shard_map/far_keys_values/pallas_call | solution.py:251
  4.2 0.0 copy-start.1
  4.2 5.3 %collective-permute-start = (bf16[2,256,128]{2,1,0:T(8,128)(2,1)}, bf16[2,256,128]{2,1,0:T(8,128)(2,1)S(1)}, u32[]{:S(2)}, u32[]{:S(2)}) collective-permute-start(bf16[2,256,128]{2,1,0:T(8,128)(2,1)} %far_keys_values.1), channel_id=1, source_target_pairs={{32,96},{40,104},{48,112},{56,120},{64,0},{72,8},{80,16},{88,24},{... | collective-permute-start | bytes 393224 | tf_op jit(solution)/shard_map/ppermute | solution.py:271
  9.5 6.0 %projections.1 = (bf16[256,128]{1,0:T(8,128)(2,1)}, bf16[2,256,128]{2,1,0:T(8,128)(2,1)}, bf16[2,256,128]{2,1,0:T(8,128)(2,1)}, bf16[2,320,128]{2,1,0:T(8,128)(2,1)}, bf16[2,320,128]{2,1,0:T(8,128)(2,1)}) custom-call(bf16[256,2048]{1,0:T(8,128)(2,1)} %tok.3, bf16[3,2048,128]{2,1,0:T(8,128)(2,1)} %wq.1, bf16[3,2048,128]{2,1,0:T(8,128)(2,1)} %wk.3, ...), custom_call_target="tpu_custom_call" | custom-call | flops 939524096 | bytes 5242880 | tf_op jit(solution)/shard_map/projections/pallas_call | solution.py:282
  15.5 0.0 copy-start.3
  15.5 0.0 copy-start.4
  15.5 0.0 collective-permute-done
  15.6 0.0 copy-done.1
  15.6 0.9 %pad_maximum_fusion = bf16[5,8,32,128]{3,2,0,1:T(8,128)(2,1)S(1)} fusion(bf16[1,8,32,128]{3,2,0,1:T(8,128)(2,1)} %bitcast.19, bf16[2,8,32,128]{3,2,1,0:T(8,128)(2,1)S(1)} %bitcast.16, bf16[2,8,32,128]{3,2,1,0:T(8,128)(2,1)S(1)} %bitcast.18), kind=kLoop, calls=%fused_computation.1 | loop fusion | flops 983040 | bytes 655360 | tf_op jit(solution)/shard_map/concatenate | solution.py:303
  16.5 14.6 %all_to_all.10.parts = bf16[8,160,128]{2,1,0:T(8,128)(2,1)} all-to-all(bf16[8,160,128]{2,1,0:T(8,128)(2,1)S(1)} %bitcast.15), channel_id=1, replica_groups={{0,8,16,24,32,40,48,56},{64,72,80,88,96,104,112,120},{128,136,144,152,1..., dimensions={0} | all-to-all | bytes 655360 | tf_op jit(solution)/shard_map/all_to_all | solution.py:306
  31.1 2.3 %far_attention.1 = bf16[8,64,128]{2,1,0:T(8,128)(2,1)} custom-call(bf16[8,160,128]{2,1,0:T(8,128)(2,1)} %all_to_all.10.parts), custom_call_target="tpu_custom_call" | custom-call | flops 134217728 | bytes 524288 | tf_op jit(solution)/shard_map/far_attention/pallas_call | solution.py:308
  33.4 6.4 %all-to-all-start.1 = ((bf16[8,64,128]{2,1,0:T(8,128)(2,1)}), bf16[8,64,128]{2,1,0:T(8,128)(2,1)S(1)}, u32[]{:S(2)}, u32[]{:S(2)}) async-start(bf16[8,64,128]{2,1,0:T(8,128)(2,1)} %far_attention.1), calls=%async_computation.1 | async-start | bytes 262144 | tf_op jit(solution)/shard_map/all_to_all | solution.py:316
  39.9 0.0 copy-done.3
  39.9 3.8 %collective-permute-start.1 = (bf16[2,320,128]{2,1,0:T(8,128)(2,1)S(1)}, bf16[2,320,128]{2,1,0:T(8,128)(2,1)S(1)}, u32[]{:S(2)}, u32[]{:S(2)}) collective-permute-start(bf16[2,320,128]{2,1,0:T(8,128)(2,1)S(1)} %copy-done.3), channel_id=1, source_target_pairs={{0,8},{8,16},{16,24},{24,32},{32,40},{40,48},{48,56},{56,64},{64,7... | collective-permute-start | bytes 491528 | tf_op jit(solution)/shard_map/ppermute | solution.py:299
  43.7 0.0 copy-done.4
  43.7 1.9 %collective-permute-start.2 = (bf16[2,320,128]{2,1,0:T(8,128)(2,1)S(1)}, bf16[2,320,128]{2,1,0:T(8,128)(2,1)S(1)}, u32[]{:S(2)}, u32[]{:S(2)}) collective-permute-start(bf16[2,320,128]{2,1,0:T(8,128)(2,1)S(1)} %copy-done.4), channel_id=1, source_target_pairs={{8,0},{16,8},{24,16},{32,24},{40,32},{48,40},{56,48},{64,56},{72,6... | collective-permute-start | bytes 491528 | tf_op jit(solution)/shard_map/ppermute | solution.py:300
  45.6 2.0 %collective-permute-done.1.low = bf16[2,320,128]{2,1,0:T(8,128)(2,1)S(1)} collective-permute-done((bf16[2,320,128]{2,1,0:T(8,128)(2,1)S(1)}, bf16[2,320,128]{2,1,0:T(8,128)(2,1)S(1)}, u32[]{:S(2)}, u32[]{:S(2)}) %collective-permute-start.1) | collective-permute-done | bytes 163872 | tf_op jit(solution)/shard_map/ppermute | solution.py:299
  47.6 0.0 copy-start.5
  47.6 5.4 %collective-permute-done.2.high = bf16[2,320,128]{2,1,0:T(8,128)(2,1)S(1)} collective-permute-done((bf16[2,320,128]{2,1,0:T(8,128)(2,1)S(1)}, bf16[2,320,128]{2,1,0:T(8,128)(2,1)S(1)}, u32[]{:S(2)}, u32[]{:S(2)}) %collective-permute-start.2) | collective-permute-done | bytes 163872 | tf_op jit(solution)/shard_map/ppermute | solution.py:300
  53.1 0.0 copy-start.6
  53.1 0.0 copy-done.5
  53.1 0.7 copy-done.6
  53.7 2.9 %near_attention.1 = (f32[256,128]{1,0:T(8,128)}, f32[256,128]{1,0:T(8,128)}) custom-call(bf16[2,256,128]{2,1,0:T(8,128)(2,1)} %get-tuple-element.13.q12, bf16[2,256,128]{2,1,0:T(8,128)(2,1)} %get-tuple-element.14.kv1, bf16[2,320,128]{2,1,0:T(8,128)(2,1)} %get-tuple-element.15.up, bf16[2,320,128]{2,1,0:T(8,128)(2,1)} %copy-done.5, bf16[2,320,128]{2,1,0:T(8,128)(2,1)} %copy-done.6), custom_call_target="tpu_custom_call" | custom-call | flops 268435456 | bytes 1048576 | tf_op jit(solution)/shard_map/near_attention/pallas_call | solution.py:319
  56.6 0.0 all-to-all-done.1.parts
  56.6 0.0 copy-start.2
  56.6 0.7 copy-done.2
  57.3 1.9 %merge.1 = bf16[256,128]{1,0:T(8,128)(2,1)} custom-call(bf16[8,64,128]{2,1,0:T(8,128)(2,1)} %copy-done.2, f32[256,128]{1,0:T(8,128)} %get-tuple-element.17.out12, f32[256,128]{1,0:T(8,128)} %get-tuple-element.18.lse12), custom_call_target="tpu_custom_call" | custom-call | flops 1048576 | bytes 524288 | tf_op jit(solution)/shard_map/merge/pallas_call | solution.py:329
  59.1 17.6 %all-gather = bf16[2048,128]{1,0:T(8,128)(2,1)S(1)} all-gather(bf16[256,128]{1,0:T(8,128)(2,1)} %merge.1), channel_id=2, replica_groups=mesh['sp'=96,'tp'=8] {'tp'}, dimensions={0}, use_global_device_ids=true | all-gather | bytes 589824 | tf_op jit(solution)/shard_map/all_gather | solution.py:339
  76.7 0.2 copy.14
  77.0 0.0 copy-done
  77.0 1.0 %convolution_convert_fusion = bf16[256,256]{1,0:T(8,128)(2,1)} fusion(bf16[256,1024]{0,1:T(8,128)(2,1)S(1)} %bitcast.17, bf16[1024,256]{1,0:T(8,128)(2,1)S(1)} %copy-done), kind=kOutput, calls=%fused_computation | convolution fusion | flops 134283264 | bytes 1179648 | tf_op jit(solution)/shard_map/dot_general | solution.py:341
Async XLA Ops:
  0.0 77.0 %copy-start = (bf16[1024,256]{1,0:T(8,128)(2,1)S(1)}, bf16[1024,256]{1,0:T(8,128)(2,1)}, u32[]{:S(2)}) copy-start(bf16[1024,256]{1,0:T(8,128)(2,1)} %param.11) | copy-start | bytes 1572868
  4.2 11.4 %copy-start.1 = (bf16[2,256,128]{2,1,0:T(8,128)(2,1)S(1)}, bf16[2,256,128]{2,1,0:T(8,128)(2,1)}, u32[]{:S(2)}) copy-start(bf16[2,256,128]{2,1,0:T(8,128)(2,1)} %far_keys_values.1) | copy-start | bytes 393220
  4.2 11.4 %collective-permute-start = (bf16[2,256,128]{2,1,0:T(8,128)(2,1)}, bf16[2,256,128]{2,1,0:T(8,128)(2,1)S(1)}, u32[]{:S(2)}, u32[]{:S(2)}) collective-permute-start(bf16[2,256,128]{2,1,0:T(8,128)(2,1)} %far_keys_values.1), channel_id=1, source_target_pairs={{32,96},{40,104},{48,112},{56,120},{64,0},{72,8},{80,16},{88,24},{... | collective-permute-start | bytes 393224 | tf_op jit(solution)/shard_map/ppermute | solution.py:271
  15.5 24.3 %copy-start.3 = (bf16[2,320,128]{2,1,0:T(8,128)(2,1)S(1)}, bf16[2,320,128]{2,1,0:T(8,128)(2,1)}, u32[]{:S(2)}) copy-start(bf16[2,320,128]{2,1,0:T(8,128)(2,1)} %get-tuple-element.15.up) | copy-start | bytes 491524
  15.5 28.1 %copy-start.4 = (bf16[2,320,128]{2,1,0:T(8,128)(2,1)S(1)}, bf16[2,320,128]{2,1,0:T(8,128)(2,1)}, u32[]{:S(2)}) copy-start(bf16[2,320,128]{2,1,0:T(8,128)(2,1)} %get-tuple-element.16) | copy-start | bytes 491524
  33.4 23.2 %all-to-all-start.1 = ((bf16[8,64,128]{2,1,0:T(8,128)(2,1)}), bf16[8,64,128]{2,1,0:T(8,128)(2,1)S(1)}, u32[]{:S(2)}, u32[]{:S(2)}) async-start(bf16[8,64,128]{2,1,0:T(8,128)(2,1)} %far_attention.1), calls=%async_computation.1 | async-start | bytes 262144 | tf_op jit(solution)/shard_map/all_to_all | solution.py:316
  39.9 7.7 %collective-permute-start.1 = (bf16[2,320,128]{2,1,0:T(8,128)(2,1)S(1)}, bf16[2,320,128]{2,1,0:T(8,128)(2,1)S(1)}, u32[]{:S(2)}, u32[]{:S(2)}) collective-permute-start(bf16[2,320,128]{2,1,0:T(8,128)(2,1)S(1)} %copy-done.3), channel_id=1, source_target_pairs={{0,8},{8,16},{16,24},{24,32},{32,40},{40,48},{48,56},{56,64},{64,7... | collective-permute-start | bytes 491528 | tf_op jit(solution)/shard_map/ppermute | solution.py:299
  43.7 9.4 %collective-permute-start.2 = (bf16[2,320,128]{2,1,0:T(8,128)(2,1)S(1)}, bf16[2,320,128]{2,1,0:T(8,128)(2,1)S(1)}, u32[]{:S(2)}, u32[]{:S(2)}) collective-permute-start(bf16[2,320,128]{2,1,0:T(8,128)(2,1)S(1)} %copy-done.4), channel_id=1, source_target_pairs={{8,0},{16,8},{24,16},{32,24},{40,32},{48,40},{56,48},{64,56},{72,6... | collective-permute-start | bytes 491528 | tf_op jit(solution)/shard_map/ppermute | solution.py:300
  47.6 5.5 %copy-start.5 = (bf16[2,320,128]{2,1,0:T(8,128)(2,1)}, bf16[2,320,128]{2,1,0:T(8,128)(2,1)S(1)}, u32[]{:S(2)}) copy-start(bf16[2,320,128]{2,1,0:T(8,128)(2,1)S(1)} %collective-permute-done.1.low) | copy-start | bytes 491524
  53.1 0.7 copy-start.6
  56.6 0.7 copy-start.2

commit v2 on v1

--- a/solution.py
+++ b/solution.py
@@ -7,6 +7,7 @@
 from jax.experimental import pallas as pl
 from jax.experimental.pallas import tpu as pltpu
 from jax.sharding import PartitionSpec as P
+
 
 HEAD_DIM = 64
 SIDE = 64
@@ -16,7 +17,7 @@
 ROW = 8
 BF = jnp.bfloat16
 F32 = jnp.float32
-SPLIT = 4
+PIECES = 2
 
 
 def rotary_tables(devices, length):
@@ -57,59 +58,95 @@
         out[pl.ds(c * n, n), :] = scratch[pl.ds(c, n, stride=dilation), :].astype(BF)
 
 
-def far_kernel(tok, wk, wv, far, near, out, acc, scratch):
-    step = pl.program_id(0)
-
-    @pl.when(step == 0)
-    def _():
-        acc[...] = jnp.zeros_like(acc)
-
-    x = tok[...]
-    acc[0] += jnp.dot(x, wk[0], preferred_element_type=F32)
-    acc[1] += jnp.dot(x, wv[0], preferred_element_type=F32)
-
-    @pl.when(step == SPLIT - 1)
-    def _():
-        tables = turn_tables(far, near)
-        store_by_class(rotate(acc[0], tables), scratch.at[0], out.at[0], FAR)
-        store_by_class(acc[1], scratch.at[1], out.at[1], FAR)
-
-
-def rest_kernel(tok, wq, wk, wv, far, near, q3, q12, kv1, up, down, acc, scratch):
-    step = pl.program_id(0)
-
-    @pl.when(step == 0)
-    def _():
-        acc[...] = jnp.zeros_like(acc)
-
-    x = tok[...]
-    for g in range(3):
-        acc[g] += jnp.dot(x, wq[g], preferred_element_type=F32)
-    for g in range(2):
-        acc[3 + g] += jnp.dot(x, wk[g], preferred_element_type=F32)
-        acc[5 + g] += jnp.dot(x, wv[g], preferred_element_type=F32)
-
-    @pl.when(step == SPLIT - 1)
-    def _():
-        length = tok.shape[0]
-        tables = turn_tables(far, near)
-        store_by_class(rotate(acc[2], tables), scratch.at[0], q3, FAR)
-        q12[0] = rotate(acc[0], tables).astype(BF)
-        store_by_class(rotate(acc[1], tables), scratch.at[1], q12.at[1], MIDDLE)
-        k1 = rotate(acc[3], tables).astype(BF)
-        v1 = acc[5].astype(BF)
-        for n, x1 in enumerate((k1, v1)):
-            kv1[n] = x1
-            up[n, pl.ds(length, SIDE), :] = x1[length - SIDE :]
-            down[n, pl.ds(length, SIDE), :] = x1[:SIDE]
-        middle = (rotate(acc[4], tables), acc[6])
+def fetch(tok, tok_buf, weights, buf, sem):
+    width = tok.shape[1] // PIECES
+    rows = buf.shape[0] // PIECES
+    copies = []
+    for p in range(PIECES):
+        at = pl.ds(p * width, width)
+        copies.append(pltpu.make_async_copy(tok.at[:, at], tok_buf.at[:, at], sem.at[p]))
+        copies[-1].start()
+        if p == 0:
+            for n, (ref, group) in enumerate(weights[:2]):
+                for q in range(PIECES):
+                    part = pl.ds(q * rows, rows)
+                    copy = pltpu.make_async_copy(
+                        ref.at[group, part, :],
+                        buf.at[part, pl.ds(n * LANES, LANES)],
+                        sem.at[PIECES + n * PIECES + q],
+                    )
+                    copies.append(copy)
+    for q in range(PIECES):
         for n in range(2):
-            scratch[2 + n] = middle[n]
-            rows = length // MIDDLE
-            for c in range(MIDDLE):
-                part = scratch[2 + n, pl.ds(c, rows, stride=MIDDLE), :].astype(BF)
-                up[n, pl.ds(c * rows, rows), :] = part
-                down[n, pl.ds(c * rows, rows), :] = part
+            copies[1 + n * PIECES + q].start()
+    rest = []
+    for n, (ref, group) in enumerate(weights[2:], 2):
+        rest.append(
+            pltpu.make_async_copy(
+                ref.at[group], buf.at[:, pl.ds(n * LANES, LANES)], sem.at[PIECES * 3 + n - 2]
+            )
+        )
+        rest[-1].start()
+    tokens = [copies[0]] + copies[1 + 2 * PIECES :]
+    return tokens, [[copies[1 + n * PIECES + q] for n in range(2)] for q in range(PIECES)], rest
+
+
+def first_pair(tok_buf, buf, copies):
+    tokens, pair, _ = copies
+    total = None
+    width = tok_buf.shape[1] // PIECES
+    for p in range(PIECES):
+        tokens[p].wait()
+        for copy in pair[p]:
+            copy.wait()
+        at = pl.ds(p * width, width)
+        part = jnp.dot(tok_buf[:, at], buf[at, : 2 * LANES], preferred_element_type=F32)
+        total = part if total is None else total + part
+    return total
+
+
+def far_kernel(tok, wk, wv, far, near, out, tok_buf, buf, scratch, sem):
+    copies = fetch(tok, tok_buf, ((wk, 2), (wv, 2)), buf, sem)
+    tables = turn_tables(far, near)
+    both = first_pair(tok_buf, buf, copies)
+    store_by_class(rotate(both[:, :LANES], tables), scratch.at[0], out.at[0], FAR)
+    store_by_class(both[:, LANES:], scratch.at[1], out.at[1], FAR)
+
+
+def rest_kernel(
+    tok, wq, wk, wv, far, near, q3, q12, kv1, up, down, tok_buf, buf, scratch, sem
+):
+    length = tok.shape[0]
+    weights = ((wk, 1), (wv, 1), (wk, 0), (wv, 0), (wq, 2), (wq, 1), (wq, 0))
+    copies = fetch(tok, tok_buf, weights, buf, sem)
+    tables = turn_tables(far, near)
+    both = first_pair(tok_buf, buf, copies)
+    rest = copies[2]
+    rows = length // MIDDLE
+    for n, x2 in enumerate((rotate(both[:, :LANES], tables), both[:, LANES:])):
+        scratch[n] = x2
+        for c in range(MIDDLE):
+            part = scratch[n, pl.ds(c, rows, stride=MIDDLE), :].astype(BF)
+            up[n, pl.ds(c * rows, rows), :] = part
+            down[n, pl.ds(c * rows, rows), :] = part
+    x = tok_buf[...]
+
+    def project(n, count):
+        for m in range(count):
+            rest[n - 2 + m].wait()
+        at = pl.ds(n * LANES, count * LANES)
+        return jnp.dot(x, buf[:, at], preferred_element_type=F32)
+
+    both = project(2, 2)
+    for n, x1 in enumerate((rotate(both[:, :LANES], tables), both[:, LANES:])):
+        x1 = x1.astype(BF)
+        kv1[n] = x1
+        up[n, pl.ds(length, SIDE), :] = x1[length - SIDE :]
+        down[n, pl.ds(length, SIDE), :] = x1[:SIDE]
+    both = project(4, 2)
+    store_by_class(rotate(both[:, :LANES], tables), scratch.at[2], q3, FAR)
+    store_by_class(rotate(both[:, LANES:], tables), scratch.at[3], q12.at[1], MIDDLE)
+    q12[0] = rotate(project(6, 1), tables).astype(BF)
 
 
 def attend(q, k, v, low, high):
@@ -233,6 +270,10 @@
     return pl.BlockSpec(memory_space=pltpu.VMEM)
 
 
+def room(mib):
+    return pltpu.CompilerParams(vmem_limit_bytes=mib << 20)
+
+
 def cost(flops, size):
     return pl.CostEstimate(flops=flops, bytes_accessed=size, transcendentals=0)
 
@@ -241,24 +282,20 @@
     length, width = tokens.shape
     columns = key_weight.shape[2]
     far, near = rotary_tables(devices, length)
-    chunk = width // SPLIT
-    fixed = [
-        pl.BlockSpec(far.shape, lambda k: (0, 0)),
-        pl.BlockSpec(near.shape, lambda k: (0, 0, 0)),
-    ]
-    token_spec = pl.BlockSpec((length, chunk), lambda k: (0, k))
-    one = pl.BlockSpec((1, chunk, columns), lambda k: (2, k, 0))
+    hbm = pl.BlockSpec(memory_space=pltpu.HBM)
     kv3 = pl.pallas_call(
         far_kernel,
-        grid=(SPLIT,),
-        in_specs=[token_spec, one, one] + fixed,
-        out_specs=pl.BlockSpec((2, length, columns), lambda k: (0, 0, 0)),
+        in_specs=[hbm, hbm, hbm, whole(), whole()],
+        out_specs=whole(),
         out_shape=vmem((2, length, columns)),
         scratch_shapes=[
+            pltpu.VMEM((length, width), BF),
+            pltpu.VMEM((width, 2 * columns), BF),
             pltpu.VMEM((2, length, columns), F32),
-            pltpu.VMEM((2, length, columns), F32),
+            pltpu.SemaphoreType.DMA((3 * PIECES,)),
         ],
         cost_estimate=cost(4 * length * width * columns, 2 << 20),
+        compiler_params=room(63),
         name="far_keys_values",
     )(tokens, key_weight, value_weight, far, near)
 
@@ -270,7 +307,6 @@
             route.append((s, target))
     halo3 = lax.ppermute(kv3, "sp", route)
 
-    two = pl.BlockSpec((2, chunk, columns), lambda k: (0, k, 0))
     edge = length + SIDE
     shapes = [
         (length, columns),
@@ -281,18 +317,17 @@
     ]
     q3, q12, kv1, up, down = pl.pallas_call(
         rest_kernel,
-        grid=(SPLIT,),
-        in_specs=[token_spec, pl.BlockSpec((3, chunk, columns), lambda k: (0, k, 0)), two, two]
-        + fixed,
-        out_specs=[
-            pl.BlockSpec(s, functools.partial(lambda n, k: (0,) * n, len(s))) for s in shapes
-        ],
+        in_specs=[hbm, hbm, hbm, hbm, whole(), whole()],
+        out_specs=[whole()] * len(shapes),
         out_shape=[vmem(s) for s in shapes],
         scratch_shapes=[
-            pltpu.VMEM((7, length, columns), F32),
+            pltpu.VMEM((length, width), BF),
+            pltpu.VMEM((width, 7 * columns), BF),
             pltpu.VMEM((4, length, columns), F32),
+            pltpu.SemaphoreType.DMA((3 * PIECES + 5,)),
         ],
         cost_estimate=cost(14 * length * width * columns, 5 << 20),
+        compiler_params=room(63),
         name="projections",
     )(tokens, query_weight, key_weight, value_weight, far, near)
 
@@ -311,6 +346,7 @@
         out_specs=whole(),
         out_shape=vmem((ROW, 2 * size, columns)),
         cost_estimate=cost(1 << 27, 1 << 19),
+        compiler_params=room(4),
         name="far_attention",
     )(parts)
     parts3 = lax.all_to_all(back, "sp", 0, 0, axis_index_groups=groups, tiled=True)
@@ -323,6 +359,7 @@
         out_shape=[flat, flat],
         scratch_shapes=[pltpu.VMEM((length, columns), F32)] * 2,
         cost_estimate=cost(1 << 28, 1 << 20),
+        compiler_params=room(6),
         name="near_attention",
     )(q12, kv1, up, low, high)
 
@@ -333,6 +370,7 @@
         out_shape=vmem((length, columns)),
         scratch_shapes=[pltpu.VMEM((length, columns), F32)] * 2,
         cost_estimate=cost(1 << 20, 1 << 19),
+        compiler_params=room(2),
         name="merge",
     )(parts3, out12, lse12)
 
@@ -344,8 +382,12 @@
 
 def solution(mesh):
     weights = P(None, None, "tp")
+
+    def body(*args):
+        return per_device(mesh.shape["sp"], *args)
+
     return jax.shard_map(
-        functools.partial(per_device, mesh.shape["sp"]),
+        body,
         mesh=mesh,
         in_specs=(P("sp", None), weights, weights, weights, P(None, "tp")),
         out_specs=P("sp", "tp"),

time: 78.5 us -> 72.6 us (0.925)
  Pallas kernels: 17.3 us -> 12.9 us
  local copies, waits for them, and re-layouts: 1.55 us -> 0.24 us
    pallas_call x1, Pallas kernels: 2.88 us -> 0.98 us  [per_device(): pl.pallas_call(functools.partial(near_attention_kernel, devices), in_spec...]
    pallas_call x1, Pallas kernels: 1.87 us -> 0.21 us  [per_device(): pl.pallas_call(merge_kernel, in_specs=[whole()] * 3, out_specs=whole(), o...]
    unnamed x14 -> x10, local copies, waits for them, and re-layouts: 1.34 us -> 0.02 us
    pallas_call x1, Pallas kernels: 2.32 us -> 1.34 us  [per_device(): pl.pallas_call(functools.partial(far_attention_kernel, devices // ROW), i...]
  transfers between devices with their start and end apart: 4 -> 4, of which waited for: 2 -> 2; matrix products, arithmetic and copies ran while one was open for 0% -> 0% of each run, Pallas kernels for 11% -> 10%
where the time goes in v2:
time: 72.6 us; the launch traced here: 72.2 us
  blocking collectives  31.9 us (44%)
  starting transfers between devices  17.4 us (24%)
  Pallas kernels  12.9 us (18%)
  waiting for transfers between devices  7.46 us (10%)
  other arithmetic  1.1 us (2%)
  matrix products  1.01 us (1%)
    all_gather x1, blocking collectives, per_device(): gathered = lax.all_gather(merged, 'tp', axis=0, tiled=False)  17.4 us
    all_to_all x1, blocking collectives, per_device(): lax.all_to_all(packed, 'sp', 0, 0, axis_index_groups=groups, tiled=True)  14.5 us
    pallas_call x1, Pallas kernels, per_device(): pl.pallas_call(rest_kernel, in_specs=[hbm, hbm, hbm, hbm, whole(), whole(...  6.58 us
    all_to_all x1, starting transfers between devices, per_device(): lax.all_to_all(back, 'sp', 0, 0, axis_index_groups=groups, tiled=True)  6.44 us
    ppermute x1, waiting for transfers between devices, per_device(): high = lax.ppermute(down, 'sp', [(s + 1, s) for s in range(devices - 1)])  5.44 us
    ppermute x1, starting transfers between devices, per_device(): halo3 = lax.ppermute(kv3, 'sp', route)  5.21 us
    pallas_call x1, Pallas kernels, per_device(): pl.pallas_call(far_kernel, in_specs=[hbm, hbm, hbm, whole(), whole()], ou...  3.84 us
    ppermute x1, starting transfers between devices, per_device(): low = lax.ppermute(up, 'sp', [(s, s + 1) for s in range(devices - 1)])  3.79 us
  transfers between devices with their start and end apart: 4, of which 2 were waited for; matrix products, arithmetic and copies ran while one was open for 0% of the time, Pallas kernels for 10%

profile of v2, /device:TPU:249, one launch (start us, length us, event | category | flops | bytes accessed | tf_op | source)
XLA Modules:
  0.0 72.2 jit_solution(3745550753923754698)
XLA Ops:
  0.0 0.0 copy-start
  0.0 3.8 %far_keys_values.1 = bf16[2,256,128]{2,1,0:T(8,128)(2,1)} custom-call(bf16[256,2048]{1,0:T(8,128)(2,1)} %tok.3, bf16[3,2048,128]{2,1,0:T(8,128)(2,1)} %wk.3, bf16[3,2048,128]{2,1,0:T(8,128)(2,1)} %wv.3, f32[96,512]{1,0:T(8,128)} %constant.4.clone.far, f32[2,256,128]{2,1,0:T(8,128)} %constant.5.clone.near), custom_call_target="tpu_custom_call" | custom-call | flops 268435456 | bytes 2097152 | tf_op jit(solution)/shard_map/far_keys_values/pallas_call | solution.py:286
  3.9 5.2 %collective-permute-start = (bf16[2,256,128]{2,1,0:T(8,128)(2,1)}, bf16[2,256,128]{2,1,0:T(8,128)(2,1)}, u32[]{:S(2)}, u32[]{:S(2)}) collective-permute-start(bf16[2,256,128]{2,1,0:T(8,128)(2,1)} %far_keys_values.1), channel_id=1, source_target_pairs={{32,96},{40,104},{48,112},{56,120},{64,0},{72,8},{80,16},{88,24},{... | collective-permute-start | bytes 393224 | tf_op jit(solution)/shard_map/ppermute | solution.py:308
  9.1 6.6 %projections.1 = (bf16[256,128]{1,0:T(8,128)(2,1)}, bf16[2,256,128]{2,1,0:T(8,128)(2,1)}, bf16[2,256,128]{2,1,0:T(8,128)(2,1)}, bf16[2,320,128]{2,1,0:T(8,128)(2,1)}, bf16[2,320,128]{2,1,0:T(8,128)(2,1)}) custom-call(bf16[256,2048]{1,0:T(8,128)(2,1)} %tok.3, bf16[3,2048,128]{2,1,0:T(8,128)(2,1)} %wq.1, bf16[3,2048,128]{2,1,0:T(8,128)(2,1)} %wk.3, ...), custom_call_target="tpu_custom_call" | custom-call | flops 939524096 | bytes 5242880 | tf_op jit(solution)/shard_map/projections/pallas_call | solution.py:318
  15.7 0.0 copy-start.1
  15.7 0.0 copy-start.4
  15.7 0.0 copy-start.2
  15.7 0.0 copy-start.3
  15.7 0.0 collective-permute-done
  15.7 1.1 %pad_maximum_fusion = bf16[5,8,32,128]{3,2,0,1:T(8,128)(2,1)S(1)} fusion(bf16[1,8,32,128]{3,2,0,1:T(8,128)(2,1)} %bitcast.18, bf16[2,8,32,128]{3,2,1,0:T(8,128)(2,1)} %bitcast.16, bf16[2,8,32,128]{3,2,1,0:T(8,128)(2,1)} %bitcast.3), kind=kLoop, calls=%fused_computation.1 | loop fusion | flops 983040 | bytes 655360 | tf_op jit(solution)/shard_map/concatenate | solution.py:338
  16.8 14.5 %all_to_all.10.parts = bf16[8,160,128]{2,1,0:T(8,128)(2,1)S(1)} all-to-all(bf16[8,160,128]{2,1,0:T(8,128)(2,1)S(1)} %bitcast.15), channel_id=1, replica_groups={{0,8,16,24,32,40,48,56},{64,72,80,88,96,104,112,120},{128,136,144,152,1..., dimensions={0} | all-to-all | bytes 655360 | tf_op jit(solution)/shard_map/all_to_all | solution.py:341
  31.3 1.3 %far_attention.1 = bf16[8,64,128]{2,1,0:T(8,128)(2,1)} custom-call(bf16[8,160,128]{2,1,0:T(8,128)(2,1)S(1)} %all_to_all.10.parts), custom_call_target="tpu_custom_call" | custom-call | flops 134217728 | bytes 524288 | tf_op jit(solution)/shard_map/far_attention/pallas_call | solution.py:343
  32.7 6.4 %all-to-all-start.1 = ((bf16[8,64,128]{2,1,0:T(8,128)(2,1)}), bf16[8,64,128]{2,1,0:T(8,128)(2,1)S(1)}, u32[]{:S(2)}, u32[]{:S(2)}) async-start(bf16[8,64,128]{2,1,0:T(8,128)(2,1)} %far_attention.1), calls=%async_computation.1 | async-start | bytes 262144 | tf_op jit(solution)/shard_map/all_to_all | solution.py:352
  39.1 0.0 copy-done.1
  39.1 3.8 %collective-permute-start.1 = (bf16[2,320,128]{2,1,0:T(8,128)(2,1)S(1)}, bf16[2,320,128]{2,1,0:T(8,128)(2,1)S(1)}, u32[]{:S(2)}, u32[]{:S(2)}) collective-permute-start(bf16[2,320,128]{2,1,0:T(8,128)(2,1)S(1)} %copy-done.1), channel_id=1, source_target_pairs={{0,8},{8,16},{16,24},{24,32},{32,40},{40,48},{48,56},{56,64},{64,7... | collective-permute-start | bytes 491528 | tf_op jit(solution)/shard_map/ppermute | solution.py:334
  42.9 0.0 copy-done.4
  42.9 1.9 %collective-permute-start.2 = (bf16[2,320,128]{2,1,0:T(8,128)(2,1)S(1)}, bf16[2,320,128]{2,1,0:T(8,128)(2,1)S(1)}, u32[]{:S(2)}, u32[]{:S(2)}) collective-permute-start(bf16[2,320,128]{2,1,0:T(8,128)(2,1)S(1)} %copy-done.4), channel_id=1, source_target_pairs={{8,0},{16,8},{24,16},{32,24},{40,32},{48,40},{56,48},{64,56},{72,6... | collective-permute-start | bytes 491528 | tf_op jit(solution)/shard_map/ppermute | solution.py:335
  44.8 2.0 %collective-permute-done.1.low = bf16[2,320,128]{2,1,0:T(8,128)(2,1)S(1)} collective-permute-done((bf16[2,320,128]{2,1,0:T(8,128)(2,1)S(1)}, bf16[2,320,128]{2,1,0:T(8,128)(2,1)S(1)}, u32[]{:S(2)}, u32[]{:S(2)}) %collective-permute-start.1) | collective-permute-done | bytes 163872 | tf_op jit(solution)/shard_map/ppermute | solution.py:334
  46.9 5.4 %collective-permute-done.2.high = bf16[2,320,128]{2,1,0:T(8,128)(2,1)S(1)} collective-permute-done((bf16[2,320,128]{2,1,0:T(8,128)(2,1)S(1)}, bf16[2,320,128]{2,1,0:T(8,128)(2,1)S(1)}, u32[]{:S(2)}, u32[]{:S(2)}) %collective-permute-start.2) | collective-permute-done | bytes 163872 | tf_op jit(solution)/shard_map/ppermute | solution.py:335
  52.3 0.0 copy-done.2
  52.3 0.0 copy-done.3
  52.3 1.0 %near_attention.1 = (f32[256,128]{1,0:T(8,128)S(1)}, f32[256,128]{1,0:T(8,128)S(1)}) custom-call(bf16[2,256,128]{2,1,0:T(8,128)(2,1)S(1)} %copy-done.2, bf16[2,256,128]{2,1,0:T(8,128)(2,1)S(1)} %copy-done.3, bf16[2,320,128]{2,1,0:T(8,128)(2,1)S(1)} %copy-done.1, bf16[2,320,128]{2,1,0:T(8,128)(2,1)S(1)} %collective-permute-done.1.low, ...), custom_call_target="tpu_custom_call" | custom-call | flops 268435456 | bytes 1048576 | tf_op jit(solution)/shard_map/near_attention/pallas_call | solution.py:355
  53.3 0.0 all-to-all-done.1.parts
  53.3 0.2 merge.1
  53.5 17.4 %all-gather = bf16[2048,128]{1,0:T(8,128)(2,1)S(1)} all-gather(bf16[256,128]{1,0:T(8,128)(2,1)S(1)} %merge.1), channel_id=2, replica_groups=mesh['sp'=96,'tp'=8] {'tp'}, dimensions={0}, use_global_device_ids=true | all-gather | bytes 589824 | tf_op jit(solution)/shard_map/all_gather | solution.py:377
  70.9 0.2 copy.14
  71.2 0.0 copy-done
  71.2 1.0 %convolution_convert_fusion = bf16[256,256]{1,0:T(8,128)(2,1)} fusion(bf16[256,1024]{0,1:T(8,128)(2,1)S(1)} %bitcast.17, bf16[1024,256]{1,0:T(8,128)(2,1)S(1)} %copy-done), kind=kOutput, calls=%fused_computation | convolution fusion | flops 134283264 | bytes 1179648 | tf_op jit(solution)/shard_map/dot_general | solution.py:379
Async XLA Ops:
  0.0 71.2 %copy-start = (bf16[1024,256]{1,0:T(8,128)(2,1)S(1)}, bf16[1024,256]{1,0:T(8,128)(2,1)}, u32[]{:S(2)}) copy-start(bf16[1024,256]{1,0:T(8,128)(2,1)} %param.11) | copy-start | bytes 1572868
  3.9 11.8 %collective-permute-start = (bf16[2,256,128]{2,1,0:T(8,128)(2,1)}, bf16[2,256,128]{2,1,0:T(8,128)(2,1)}, u32[]{:S(2)}, u32[]{:S(2)}) collective-permute-start(bf16[2,256,128]{2,1,0:T(8,128)(2,1)} %far_keys_values.1), channel_id=1, source_target_pairs={{32,96},{40,104},{48,112},{56,120},{64,0},{72,8},{80,16},{88,24},{... | collective-permute-start | bytes 393224 | tf_op jit(solution)/shard_map/ppermute | solution.py:308
  15.7 23.5 %copy-start.1 = (bf16[2,320,128]{2,1,0:T(8,128)(2,1)S(1)}, bf16[2,320,128]{2,1,0:T(8,128)(2,1)}, u32[]{:S(2)}) copy-start(bf16[2,320,128]{2,1,0:T(8,128)(2,1)} %get-tuple-element.15.up) | copy-start | bytes 491524
  15.7 27.2 %copy-start.4 = (bf16[2,320,128]{2,1,0:T(8,128)(2,1)S(1)}, bf16[2,320,128]{2,1,0:T(8,128)(2,1)}, u32[]{:S(2)}) copy-start(bf16[2,320,128]{2,1,0:T(8,128)(2,1)} %get-tuple-element.16) | copy-start | bytes 491524
  15.7 36.6 %copy-start.2 = (bf16[2,256,128]{2,1,0:T(8,128)(2,1)S(1)}, bf16[2,256,128]{2,1,0:T(8,128)(2,1)}, u32[]{:S(2)}) copy-start(bf16[2,256,128]{2,1,0:T(8,128)(2,1)} %get-tuple-element.13.q12) | copy-start | bytes 393220
  15.7 36.6 %copy-start.3 = (bf16[2,256,128]{2,1,0:T(8,128)(2,1)S(1)}, bf16[2,256,128]{2,1,0:T(8,128)(2,1)}, u32[]{:S(2)}) copy-start(bf16[2,256,128]{2,1,0:T(8,128)(2,1)} %get-tuple-element.14.kv1) | copy-start | bytes 393220
  32.7 20.6 %all-to-all-start.1 = ((bf16[8,64,128]{2,1,0:T(8,128)(2,1)}), bf16[8,64,128]{2,1,0:T(8,128)(2,1)S(1)}, u32[]{:S(2)}, u32[]{:S(2)}) async-start(bf16[8,64,128]{2,1,0:T(8,128)(2,1)} %far_attention.1), calls=%async_computation.1 | async-start | bytes 262144 | tf_op jit(solution)/shard_map/all_to_all | solution.py:352
  39.1 7.7 %collective-permute-start.1 = (bf16[2,320,128]{2,1,0:T(8,128)(2,1)S(1)}, bf16[2,320,128]{2,1,0:T(8,128)(2,1)S(1)}, u32[]{:S(2)}, u32[]{:S(2)}) collective-permute-start(bf16[2,320,128]{2,1,0:T(8,128)(2,1)S(1)} %copy-done.1), channel_id=1, source_target_pairs={{0,8},{8,16},{16,24},{24,32},{32,40},{40,48},{48,56},{56,64},{64,7... | collective-permute-start | bytes 491528 | tf_op jit(solution)/shard_map/ppermute | solution.py:334
  42.9 9.4 %collective-permute-start.2 = (bf16[2,320,128]{2,1,0:T(8,128)(2,1)S(1)}, bf16[2,320,128]{2,1,0:T(8,128)(2,1)S(1)}, u32[]{:S(2)}, u32[]{:S(2)}) collective-permute-start(bf16[2,320,128]{2,1,0:T(8,128)(2,1)S(1)} %copy-done.4), channel_id=1, source_target_pairs={{8,0},{16,8},{24,16},{32,24},{40,32},{48,40},{56,48},{64,56},{72,6... | collective-permute-start | bytes 491528 | tf_op jit(solution)/shard_map/ppermute | solution.py:335

commit v3 on v2

--- a/solution.py
+++ b/solution.py
@@ -17,6 +17,7 @@
 ROW = 8
 BF = jnp.bfloat16
 F32 = jnp.float32
+GRANT = 12
 PIECES = 2
 
 
@@ -31,11 +32,10 @@
     return far.astype(np.float32), near.astype(np.float32)
 
 
-def turn_tables(far_ref, near_ref):
-    row = far_ref[pl.ds(lax.axis_index("sp"), 1), :]
+def turn_tables(row, near):
     cos_base, sin_base = row[:, :LANES], row[:, LANES : 2 * LANES]
     scos_base, ssin_base = row[:, 2 * LANES : 3 * LANES], row[:, 3 * LANES :]
-    cos_step, sin_step = near_ref[0], near_ref[1]
+    cos_step, sin_step = near[0], near[1]
     return cos_base * cos_step - sin_base * sin_step, ssin_base * cos_step + scos_base * sin_step
 
 
@@ -58,70 +58,87 @@
         out[pl.ds(c * n, n), :] = scratch[pl.ds(c, n, stride=dilation), :].astype(BF)
 
 
-def fetch(tok, tok_buf, weights, buf, sem):
-    width = tok.shape[1] // PIECES
-    rows = buf.shape[0] // PIECES
-    copies = []
-    for p in range(PIECES):
-        at = pl.ds(p * width, width)
-        copies.append(pltpu.make_async_copy(tok.at[:, at], tok_buf.at[:, at], sem.at[p]))
-        copies[-1].start()
-        if p == 0:
-            for n, (ref, group) in enumerate(weights[:2]):
-                for q in range(PIECES):
-                    part = pl.ds(q * rows, rows)
-                    copy = pltpu.make_async_copy(
-                        ref.at[group, part, :],
-                        buf.at[part, pl.ds(n * LANES, LANES)],
-                        sem.at[PIECES + n * PIECES + q],
-                    )
-                    copies.append(copy)
-    for q in range(PIECES):
-        for n in range(2):
-            copies[1 + n * PIECES + q].start()
-    rest = []
-    for n, (ref, group) in enumerate(weights[2:], 2):
-        rest.append(
-            pltpu.make_async_copy(
-                ref.at[group], buf.at[:, pl.ds(n * LANES, LANES)], sem.at[PIECES * 3 + n - 2]
+class Projector:
+    def __init__(self, tok, weights, far, near, tok_buf, buf, row_buf, near_buf, sem):
+        self.tok_buf, self.buf, self.row_buf, self.near_buf = tok_buf, buf, row_buf, near_buf
+        self.sem, self.used = sem, 0
+        width = tok.shape[1] // PIECES
+        parts = [pl.ds(p * width, width) for p in range(PIECES)]
+        self.tokens, self.first = [], []
+        for at in parts:
+            self.tokens.append(self.start(tok.at[:, at], tok_buf.at[:, at]))
+            self.first.append(
+                [
+                    self.start(ref.at[g, at, :], buf.at[at, pl.ds(n * LANES, LANES)])
+                    for n, (ref, g) in enumerate(weights[:2])
+                ]
             )
+        self.table_copies = [
+            self.start(far.at[pl.ds(lax.axis_index("sp"), 1), :], row_buf),
+            self.start(near, near_buf),
+        ]
+        self.later = [
+            self.start(ref.at[g], buf.at[:, pl.ds(n * LANES, LANES)])
+            for n, (ref, g) in enumerate(weights[2:], 2)
+        ]
+
+    def start(self, source, target):
+        copy = pltpu.make_async_copy(source, target, self.sem.at[self.used])
+        copy.start()
+        self.used += 1
+        return copy
+
+    def tables(self):
+        for copy in self.table_copies:
+            copy.wait()
+        return turn_tables(self.row_buf[...], self.near_buf)
+
+    def first_pair(self):
+        total = None
+        width = self.tok_buf.shape[1] // PIECES
+        for p in range(PIECES):
+            self.tokens[p].wait()
+            for copy in self.first[p]:
+                copy.wait()
+            at = pl.ds(p * width, width)
+            part = jnp.dot(
+                self.tok_buf[:, at], self.buf[at, : 2 * LANES], preferred_element_type=F32
+            )
+            total = part if total is None else total + part
+        return total
+
+    def product(self, n, count):
+        for m in range(count):
+            self.later[n - 2 + m].wait()
+        return jnp.dot(
+            self.tok_buf[...], self.buf[:, pl.ds(n * LANES, count * LANES)],
+            preferred_element_type=F32,
         )
-        rest[-1].start()
-    tokens = [copies[0]] + copies[1 + 2 * PIECES :]
-    return tokens, [[copies[1 + n * PIECES + q] for n in range(2)] for q in range(PIECES)], rest
-
-
-def first_pair(tok_buf, buf, copies):
-    tokens, pair, _ = copies
-    total = None
-    width = tok_buf.shape[1] // PIECES
-    for p in range(PIECES):
-        tokens[p].wait()
-        for copy in pair[p]:
-            copy.wait()
-        at = pl.ds(p * width, width)
-        part = jnp.dot(tok_buf[:, at], buf[at, : 2 * LANES], preferred_element_type=F32)
-        total = part if total is None else total + part
-    return total
-
-
-def far_kernel(tok, wk, wv, far, near, out, tok_buf, buf, scratch, sem):
-    copies = fetch(tok, tok_buf, ((wk, 2), (wv, 2)), buf, sem)
-    tables = turn_tables(far, near)
-    both = first_pair(tok_buf, buf, copies)
-    store_by_class(rotate(both[:, :LANES], tables), scratch.at[0], out.at[0], FAR)
+
+
+def projector_scratch(length, width, weights):
+    return [
+        pltpu.VMEM((length, width), BF),
+        pltpu.VMEM((width, weights * LANES), BF),
+        pltpu.VMEM((1, 4 * LANES), F32),
+        pltpu.VMEM((2, length, LANES), F32),
+        pltpu.SemaphoreType.DMA((3 * PIECES + weights,)),
+    ]
+
+
+def far_kernel(tok, wk, wv, far, near, out, scratch, *buffers):
+    work = Projector(tok, ((wk, 2), (wv, 2)), far, near, *buffers)
+    both = work.first_pair()
     store_by_class(both[:, LANES:], scratch.at[1], out.at[1], FAR)
-
-
-def rest_kernel(
-    tok, wq, wk, wv, far, near, q3, q12, kv1, up, down, tok_buf, buf, scratch, sem
-):
+    store_by_class(rotate(both[:, :LANES], work.tables()), scratch.at[0], out.at[0], FAR)
+
+
+def edges_kernel(tok, wq, wk, wv, far, near, q3, kv1, up, down, scratch, *buffers):
     length = tok.shape[0]
-    weights = ((wk, 1), (wv, 1), (wk, 0), (wv, 0), (wq, 2), (wq, 1), (wq, 0))
-    copies = fetch(tok, tok_buf, weights, buf, sem)
-    tables = turn_tables(far, near)
-    both = first_pair(tok_buf, buf, copies)
-    rest = copies[2]
+    weights = ((wk, 1), (wv, 1), (wk, 0), (wv, 0), (wq, 2))
+    work = Projector(tok, weights, far, near, *buffers)
+    both = work.first_pair()
+    tables = work.tables()
     rows = length // MIDDLE
     for n, x2 in enumerate((rotate(both[:, :LANES], tables), both[:, LANES:])):
         scratch[n] = x2
@@ -129,24 +146,21 @@
             part = scratch[n, pl.ds(c, rows, stride=MIDDLE), :].astype(BF)
             up[n, pl.ds(c * rows, rows), :] = part
             down[n, pl.ds(c * rows, rows), :] = part
-    x = tok_buf[...]
-
-    def project(n, count):
-        for m in range(count):
-            rest[n - 2 + m].wait()
-        at = pl.ds(n * LANES, count * LANES)
-        return jnp.dot(x, buf[:, at], preferred_element_type=F32)
-
-    both = project(2, 2)
+    both = work.product(2, 2)
     for n, x1 in enumerate((rotate(both[:, :LANES], tables), both[:, LANES:])):
         x1 = x1.astype(BF)
         kv1[n] = x1
         up[n, pl.ds(length, SIDE), :] = x1[length - SIDE :]
         down[n, pl.ds(length, SIDE), :] = x1[:SIDE]
-    both = project(4, 2)
-    store_by_class(rotate(both[:, :LANES], tables), scratch.at[2], q3, FAR)
-    store_by_class(rotate(both[:, LANES:], tables), scratch.at[3], q12.at[1], MIDDLE)
-    q12[0] = rotate(project(6, 1), tables).astype(BF)
+    store_by_class(rotate(work.product(4, 1), tables), scratch.at[2], q3, FAR)
+
+
+def pack_kernel(q3, kv3, halo3, packed):
+    size = packed.shape[1] // 5
+    for y in range(ROW):
+        at = pl.ds(y * size, size)
+        for n, part in enumerate((q3[at, :], kv3[0, at, :], kv3[1, at, :], halo3[0, at, :], halo3[1, at, :])):
+            packed[y, pl.ds(n * size, size), :] = part
 
 
 def attend(q, k, v, low, high):
@@ -181,8 +195,15 @@
     return (wa * out_a + wb * out_b) / total, top + jnp.log(total)
 
 
-def near_attention_kernel(devices, q12, kv1, up, low, high, out, lse, out2, lse2):
+def near_attention_kernel(
+    devices, tok, wq, far, near, kv1, up, low, high, out, lse, out2, lse2, q12, scratch, *buffers
+):
     length = kv1.shape[1]
+    work = Projector(tok, ((wq, 0), (wq, 1)), far, near, *buffers)
+    both = work.first_pair()
+    tables = work.tables()
+    q12[0] = rotate(both[:, :LANES], tables).astype(BF)
+    store_by_class(rotate(both[:, LANES:], tables), scratch, q12.at[1], MIDDLE)
     me = lax.axis_index("sp")
     rows = length // MIDDLE
     start = jnp.where(me == 0, SIDE, 0)
@@ -262,6 +283,18 @@
     merged[...] = o.astype(BF)
 
 
+def output_kernel(gathered, weight, mixed):
+    total = None
+    columns = gathered.shape[2]
+    for n in range(0, gathered.shape[0], 2):
+        pair = jnp.concatenate([gathered[n], gathered[n + 1]], axis=1)
+        part = jnp.dot(
+            pair, weight[pl.ds(n * columns, 2 * columns), :], preferred_element_type=F32
+        )
+        total = part if total is None else total + part
+    mixed[...] = total.astype(BF)
+
+
 def vmem(shape):
     return jax.ShapeDtypeStruct(shape, BF)
 
@@ -271,7 +304,7 @@
 
 
 def room(mib):
-    return pltpu.CompilerParams(vmem_limit_bytes=mib << 20)
+    return pltpu.CompilerParams(vmem_limit_bytes=int(mib * 1024) << 10)
 
 
 def cost(flops, size):
@@ -282,20 +315,22 @@
     length, width = tokens.shape
     columns = key_weight.shape[2]
     far, near = rotary_tables(devices, length)
+    stay = functools.partial(pltpu.with_memory_space_constraint, memory_space=pltpu.HBM)
+    tokens, query_weight, key_weight, value_weight, far, near = (
+        stay(x) for x in (tokens, query_weight, key_weight, value_weight, jnp.asarray(far), jnp.asarray(near))
+    )
     hbm = pl.BlockSpec(memory_space=pltpu.HBM)
+    flat = jax.ShapeDtypeStruct((length, columns), F32)
+    scratch = pltpu.VMEM((length, columns), F32)
     kv3 = pl.pallas_call(
         far_kernel,
-        in_specs=[hbm, hbm, hbm, whole(), whole()],
+        in_specs=[hbm] * 5,
         out_specs=whole(),
         out_shape=vmem((2, length, columns)),
-        scratch_shapes=[
-            pltpu.VMEM((length, width), BF),
-            pltpu.VMEM((width, 2 * columns), BF),
-            pltpu.VMEM((2, length, columns), F32),
-            pltpu.SemaphoreType.DMA((3 * PIECES,)),
-        ],
+        scratch_shapes=[pltpu.VMEM((2, length, columns), F32)]
+        + projector_scratch(length, width, 2),
         cost_estimate=cost(4 * length * width * columns, 2 << 20),
-        compiler_params=room(63),
+        compiler_params=room(GRANT),
         name="far_keys_values",
     )(tokens, key_weight, value_weight, far, near)
 
@@ -311,23 +346,18 @@
     shapes = [
         (length, columns),
         (2, length, columns),
-        (2, length, columns),
         (2, edge, columns),
         (2, edge, columns),
     ]
-    q3, q12, kv1, up, down = pl.pallas_call(
-        rest_kernel,
-        in_specs=[hbm, hbm, hbm, hbm, whole(), whole()],
+    q3, kv1, up, down = pl.pallas_call(
+        edges_kernel,
+        in_specs=[hbm] * 6,
         out_specs=[whole()] * len(shapes),
         out_shape=[vmem(s) for s in shapes],
-        scratch_shapes=[
-            pltpu.VMEM((length, width), BF),
-            pltpu.VMEM((width, 7 * columns), BF),
-            pltpu.VMEM((4, length, columns), F32),
-            pltpu.SemaphoreType.DMA((3 * PIECES + 5,)),
-        ],
-        cost_estimate=cost(14 * length * width * columns, 5 << 20),
-        compiler_params=room(63),
+        scratch_shapes=[pltpu.VMEM((3, length, columns), F32)]
+        + projector_scratch(length, width, 5),
+        cost_estimate=cost(10 * length * width * columns, 4 << 20),
+        compiler_params=room(GRANT),
         name="projections",
     )(tokens, query_weight, key_weight, value_weight, far, near)
 
@@ -335,8 +365,15 @@
     high = lax.ppermute(down, "sp", [(s + 1, s) for s in range(devices - 1)])
 
     size = length // ROW
-    packed = jnp.concatenate([q3[None], kv3, halo3], axis=0).reshape(5, ROW, size, columns)
-    packed = jnp.swapaxes(packed, 0, 1).reshape(ROW, 5 * size, columns)
+    packed = pl.pallas_call(
+        pack_kernel,
+        in_specs=[whole()] * 3,
+        out_specs=whole(),
+        out_shape=vmem((ROW, 5 * size, columns)),
+        cost_estimate=cost(1 << 20, 1 << 19),
+        compiler_params=room(2),
+        name="pack",
+    )(q3, kv3, halo3)
     groups = [[z * ROW + y for y in range(ROW)] for z in range(devices // ROW)]
     parts = lax.all_to_all(packed, "sp", 0, 0, axis_index_groups=groups, tiled=True)
 
@@ -351,33 +388,39 @@
     )(parts)
     parts3 = lax.all_to_all(back, "sp", 0, 0, axis_index_groups=groups, tiled=True)
 
-    flat = jax.ShapeDtypeStruct((length, columns), F32)
     out12, lse12 = pl.pallas_call(
         functools.partial(near_attention_kernel, devices),
-        in_specs=[whole()] * 5,
+        in_specs=[hbm] * 4 + [whole()] * 4,
         out_specs=[whole()] * 2,
         out_shape=[flat, flat],
-        scratch_shapes=[pltpu.VMEM((length, columns), F32)] * 2,
+        scratch_shapes=[scratch, scratch, pltpu.VMEM((2, length, columns), BF), scratch]
+        + projector_scratch(length, width, 2),
         cost_estimate=cost(1 << 28, 1 << 20),
-        compiler_params=room(6),
+        compiler_params=room(GRANT),
         name="near_attention",
-    )(q12, kv1, up, low, high)
+    )(tokens, query_weight, far, near, kv1, up, low, high)
 
     merged = pl.pallas_call(
         merge_kernel,
         in_specs=[whole()] * 3,
         out_specs=whole(),
         out_shape=vmem((length, columns)),
-        scratch_shapes=[pltpu.VMEM((length, columns), F32)] * 2,
+        scratch_shapes=[scratch, scratch],
         cost_estimate=cost(1 << 20, 1 << 19),
         compiler_params=room(2),
         name="merge",
     )(parts3, out12, lse12)
 
     gathered = lax.all_gather(merged, "tp", axis=0, tiled=False)
-    gathered = jnp.swapaxes(gathered, 0, 1).reshape(length, -1)
-    mixed = jnp.dot(gathered, out_weight, preferred_element_type=F32)
-    return mixed.astype(BF)
+    return pl.pallas_call(
+        output_kernel,
+        in_specs=[whole()] * 2,
+        out_specs=whole(),
+        out_shape=vmem((length, out_weight.shape[1])),
+        cost_estimate=cost(1 << 27, 1 << 20),
+        compiler_params=room(4),
+        name="output",
+    )(gathered, out_weight)
 
 
 def solution(mesh):

time: 72.6 us -> 70 us (0.964)
  other arithmetic: 1.1 us -> 0 us
  matrix products: 1.01 us -> 0 us
    pallas_call x2 -> x4, Pallas kernels: 10.4 us -> 6.94 us  [the longest x1 3.74 us: per_device(): pl.pallas_call(edges_kernel, in_specs=[hbm] * 6, out_specs=[whole()] * le...]
    pallas_call x1, Pallas kernels: 0.98 us -> 4.32 us  [per_device(): pl.pallas_call(functools.partial(near_attention_kernel, devices), in_spec...]
    concatenate x1 -> x0, other arithmetic: 1.1 us -> none  [per_device(): jnp.concatenate([q3[None], kv3, halo3], axis=0)]
    dot_general x1 -> x0, matrix products: 1.01 us -> none  [per_device(): mixed = jnp.dot(gathered, out_weight, preferred_element_type=F32)]
  transfers between devices with their start and end apart: 4 -> 4, of which waited for: 2 -> 2; matrix products, arithmetic and copies ran while one was open for 0% -> 0% of each run, Pallas kernels for 10% -> 12%
where the time goes in v3:
time: 70 us; the launch traced here: 69.7 us
  blocking collectives  32.3 us (46%)
  starting transfers between devices  17 us (24%)
  Pallas kernels  12.8 us (18%)
  waiting for transfers between devices  7.46 us (11%)
    all_gather x1, blocking collectives, per_device(): gathered = lax.all_gather(merged, 'tp', axis=0, tiled=False)  17.8 us
    all_to_all x1, blocking collectives, per_device(): lax.all_to_all(packed, 'sp', 0, 0, axis_index_groups=groups, tiled=True)  14.5 us
    all_to_all x1, starting transfers between devices, per_device(): lax.all_to_all(back, 'sp', 0, 0, axis_index_groups=groups, tiled=True)  6.45 us
    ppermute x1, starting transfers between devices, per_device(): halo3 = lax.ppermute(kv3, 'sp', route)  5.21 us
    ppermute x1, waiting for transfers between devices, per_device(): high = lax.ppermute(down, 'sp', [(s + 1, s) for s in range(devices - 1)])  5.08 us
    pallas_call x1, Pallas kernels, per_device(): pl.pallas_call(functools.partial(near_attention_kernel, devices), in_spec...  4.32 us
    pallas_call x1, Pallas kernels, per_device(): pl.pallas_call(edges_kernel, in_specs=[hbm] * 6, out_specs=[whole()] * le...  3.74 us
    ppermute x1, starting transfers between devices, per_device(): low = lax.ppermute(up, 'sp', [(s, s + 1) for s in range(devices - 1)])  3.44 us
  transfers between devices with their start and end apart: 4, of which 2 were waited for; matrix products, arithmetic and copies ran while one was open for 0% of the time, Pallas kernels for 12%

profile of v3, /device:TPU:249, one launch (start us, length us, event | category | flops | bytes accessed | tf_op | source)
XLA Modules:
  0.0 69.7 jit_solution(1496316401146728906)
XLA Ops:
  0.0 2.2 %far_keys_values.1.kv3 = bf16[2,256,128]{2,1,0:T(8,128)(2,1)S(1)} custom-call(bf16[256,2048]{1,0:T(8,128)(2,1)} %tok.5, bf16[3,2048,128]{2,1,0:T(8,128)(2,1)} %wk.3, bf16[3,2048,128]{2,1,0:T(8,128)(2,1)} %wv.3, f32[96,512]{1,0:T(8,128)} %constant.4.clone.far, f32[2,256,128]{2,1,0:T(8,128)} %constant.5.clone.near), custom_call_target="tpu_custom_call" | custom-call | flops 268435456 | bytes 2097152 | tf_op jit(solution)/shard_map/far_keys_values/pallas_call | solution.py:325
  2.2 5.2 %collective-permute-start = (bf16[2,256,128]{2,1,0:T(8,128)(2,1)S(1)}, bf16[2,256,128]{2,1,0:T(8,128)(2,1)S(1)}, u32[]{:S(2)}, u32[]{:S(2)}) collective-permute-start(bf16[2,256,128]{2,1,0:T(8,128)(2,1)S(1)} %far_keys_values.1.kv3), channel_id=1, source_target_pairs={{32,96},{40,104},{48,112},{56,120},{64,0},{72,8},{80,16},{88,24},{... | collective-permute-start | bytes 393224 | tf_op jit(solution)/shard_map/ppermute | solution.py:343
  7.4 3.7 %projections.1 = (bf16[256,128]{1,0:T(8,128)(2,1)S(1)}, bf16[2,256,128]{2,1,0:T(8,128)(2,1)S(1)}, bf16[2,320,128]{2,1,0:T(8,128)(2,1)S(1)}, bf16[2,320,128]{2,1,0:T(8,128)(2,1)S(1)}) custom-call(bf16[256,2048]{1,0:T(8,128)(2,1)} %tok.5, bf16[3,2048,128]{2,1,0:T(8,128)(2,1)} %wq.3, bf16[3,2048,128]{2,1,0:T(8,128)(2,1)} %wk.3, bf16[3,2048,128]{2,1,0:T(8,128)(2,1)} %wv.3, ...), custom_call_target="tpu_custom_call" | custom-call | flops 671088640 | bytes 4194304 | tf_op jit(solution)/shard_map/projections/pallas_call | solution.py:352
  11.2 0.0 collective-permute-done.halo3
  11.2 14.5 %all_to_all.10.parts = bf16[8,160,128]{2,1,0:T(8,128)(2,1)S(1)} all-to-all(bf16[8,160,128]{2,1,0:T(8,128)(2,1)S(1)} %pack.1), channel_id=1, replica_groups={{0,8,16,24,32,40,48,56},{64,72,80,88,96,104,112,120},{128,136,144,152,1..., dimensions={0} | all-to-all | bytes 655360 | tf_op jit(solution)/shard_map/all_to_all | solution.py:378
  25.7 1.4 %far_attention.1 = bf16[8,64,128]{2,1,0:T(8,128)(2,1)} custom-call(bf16[8,160,128]{2,1,0:T(8,128)(2,1)S(1)} %all_to_all.10.parts), custom_call_target="tpu_custom_call" | custom-call | flops 134217728 | bytes 524288 | tf_op jit(solution)/shard_map/far_attention/pallas_call | solution.py:380
  27.1 6.4 %all-to-all-start.1 = ((bf16[8,64,128]{2,1,0:T(8,128)(2,1)}), bf16[8,64,128]{2,1,0:T(8,128)(2,1)S(1)}, u32[]{:S(2)}, u32[]{:S(2)}) async-start(bf16[8,64,128]{2,1,0:T(8,128)(2,1)} %far_attention.1), calls=%async_computation.1 | async-start | bytes 262144 | tf_op jit(solution)/shard_map/all_to_all | solution.py:389
  33.5 3.4 %collective-permute-start.1 = (bf16[2,320,128]{2,1,0:T(8,128)(2,1)S(1)}, bf16[2,320,128]{2,1,0:T(8,128)(2,1)S(1)}, u32[]{:S(2)}, u32[]{:S(2)}) collective-permute-start(bf16[2,320,128]{2,1,0:T(8,128)(2,1)S(1)} %get-tuple-element.13.up), channel_id=1, source_target_pairs={{0,8},{8,16},{16,24},{24,32},{32,40},{40,48},{48,56},{56,64},{64,7... | collective-permute-start | bytes 491528 | tf_op jit(solution)/shard_map/ppermute | solution.py:364
  37.0 1.9 %collective-permute-start.2 = (bf16[2,320,128]{2,1,0:T(8,128)(2,1)S(1)}, bf16[2,320,128]{2,1,0:T(8,128)(2,1)S(1)}, u32[]{:S(2)}, u32[]{:S(2)}) collective-permute-start(bf16[2,320,128]{2,1,0:T(8,128)(2,1)S(1)} %get-tuple-element.14), channel_id=1, source_target_pairs={{8,0},{16,8},{24,16},{32,24},{40,32},{48,40},{56,48},{64,56},{72,6... | collective-permute-start | bytes 491528 | tf_op jit(solution)/shard_map/ppermute | solution.py:365
  38.9 2.4 %collective-permute-done.1.low = bf16[2,320,128]{2,1,0:T(8,128)(2,1)S(1)} collective-permute-done((bf16[2,320,128]{2,1,0:T(8,128)(2,1)S(1)}, bf16[2,320,128]{2,1,0:T(8,128)(2,1)S(1)}, u32[]{:S(2)}, u32[]{:S(2)}) %collective-permute-start.1) | collective-permute-done | bytes 163872 | tf_op jit(solution)/shard_map/ppermute | solution.py:364
  41.3 5.1 %collective-permute-done.2.high = bf16[2,320,128]{2,1,0:T(8,128)(2,1)S(1)} collective-permute-done((bf16[2,320,128]{2,1,0:T(8,128)(2,1)S(1)}, bf16[2,320,128]{2,1,0:T(8,128)(2,1)S(1)}, u32[]{:S(2)}, u32[]{:S(2)}) %collective-permute-start.2) | collective-permute-done | bytes 163872 | tf_op jit(solution)/shard_map/ppermute | solution.py:365
  46.4 0.0 copy-start
  46.4 4.3 %near_attention.1 = (f32[256,128]{1,0:T(8,128)S(1)}, f32[256,128]{1,0:T(8,128)S(1)}) custom-call(bf16[256,2048]{1,0:T(8,128)(2,1)} %tok.5, bf16[3,2048,128]{2,1,0:T(8,128)(2,1)} %wq.3, f32[96,512]{1,0:T(8,128)} %constant.4.clone.far, f32[2,256,128]{2,1,0:T(8,128)} %constant.5.clone.near, bf16[2,256,128]{2,1,0:T(8,128)(2,1)S(1)} %get-tuple-element.12.kv1, ...), custom_call_target="tpu_custom_call" | custom-call | flops 268435456 | bytes 1048576 | tf_op jit(solution)/shard_map/near_attention/pallas_call | solution.py:391
  50.7 0.0 all-to-all-done.1.parts
  50.7 0.2 merge.1
  50.9 17.8 %all-gather = bf16[2048,128]{1,0:T(8,128)(2,1)S(1)} all-gather(bf16[256,128]{1,0:T(8,128)(2,1)S(1)} %merge.1), channel_id=2, replica_groups=mesh['sp'=96,'tp'=8] {'tp'}, dimensions={0}, use_global_device_ids=true | all-gather | bytes 589824 | tf_op jit(solution)/shard_map/all_gather | solution.py:414
  68.7 0.0 copy-done
  68.7 1.0 %output.1 = bf16[256,256]{1,0:T(8,128)(2,1)} custom-call(bf16[8,256,128]{2,1,0:T(8,128)(2,1)S(1)} %bitcast.1, bf16[1024,256]{1,0:T(8,128)(2,1)S(1)} %copy-done), custom_call_target="tpu_custom_call" | custom-call | flops 134217728 | bytes 1048576 | tf_op jit(solution)/shard_map/output/pallas_call | solution.py:415
  (1 shorter events, 0.0 us)
Async XLA Ops:
  2.2 9.0 %collective-permute-start = (bf16[2,256,128]{2,1,0:T(8,128)(2,1)S(1)}, bf16[2,256,128]{2,1,0:T(8,128)(2,1)S(1)}, u32[]{:S(2)}, u32[]{:S(2)}) collective-permute-start(bf16[2,256,128]{2,1,0:T(8,128)(2,1)S(1)} %far_keys_values.1.kv3), channel_id=1, source_target_pairs={{32,96},{40,104},{48,112},{56,120},{64,0},{72,8},{80,16},{88,24},{... | collective-permute-start | bytes 393224 | tf_op jit(solution)/shard_map/ppermute | solution.py:343
  27.1 23.6 %all-to-all-start.1 = ((bf16[8,64,128]{2,1,0:T(8,128)(2,1)}), bf16[8,64,128]{2,1,0:T(8,128)(2,1)S(1)}, u32[]{:S(2)}, u32[]{:S(2)}) async-start(bf16[8,64,128]{2,1,0:T(8,128)(2,1)} %far_attention.1), calls=%async_computation.1 | async-start | bytes 262144 | tf_op jit(solution)/shard_map/all_to_all | solution.py:389
  33.5 7.7 %collective-permute-start.1 = (bf16[2,320,128]{2,1,0:T(8,128)(2,1)S(1)}, bf16[2,320,128]{2,1,0:T(8,128)(2,1)S(1)}, u32[]{:S(2)}, u32[]{:S(2)}) collective-permute-start(bf16[2,320,128]{2,1,0:T(8,128)(2,1)S(1)} %get-tuple-element.13.up), channel_id=1, source_target_pairs={{0,8},{8,16},{16,24},{24,32},{32,40},{40,48},{48,56},{56,64},{64,7... | collective-permute-start | bytes 491528 | tf_op jit(solution)/shard_map/ppermute | solution.py:364
  37.0 9.4 %collective-permute-start.2 = (bf16[2,320,128]{2,1,0:T(8,128)(2,1)S(1)}, bf16[2,320,128]{2,1,0:T(8,128)(2,1)S(1)}, u32[]{:S(2)}, u32[]{:S(2)}) collective-permute-start(bf16[2,320,128]{2,1,0:T(8,128)(2,1)S(1)} %get-tuple-element.14), channel_id=1, source_target_pairs={{8,0},{16,8},{24,16},{32,24},{40,32},{48,40},{56,48},{64,56},{72,6... | collective-permute-start | bytes 491528 | tf_op jit(solution)/shard_map/ppermute | solution.py:365
  46.4 22.3 %copy-start = (bf16[1024,256]{1,0:T(8,128)(2,1)S(1)}, bf16[1024,256]{1,0:T(8,128)(2,1)}, u32[]{:S(2)}) copy-start(bf16[1024,256]{1,0:T(8,128)(2,1)} %weight.1) | copy-start | bytes 1572868

commit v4 on v3

--- a/solution.py
+++ b/solution.py
@@ -280,16 +280,18 @@
         lse3[at, :] = parts[y, pl.ds(size + e * run, run), :].astype(F32)
     l = lse3[...]
     o, _ = merge(out12[...], lse12[...], out3[...], l + swap_halves(l))
-    merged[...] = o.astype(BF)
+    o = o.astype(BF)
+    for n in range(merged.shape[0]):
+        merged[n] = o
 
 
 def output_kernel(gathered, weight, mixed):
     total = None
-    columns = gathered.shape[2]
-    for n in range(0, gathered.shape[0], 2):
-        pair = jnp.concatenate([gathered[n], gathered[n + 1]], axis=1)
+    columns = gathered.shape[3]
+    for n in range(gathered.shape[1]):
+        pair = jnp.concatenate([gathered[0, n], gathered[1, n]], axis=1)
         part = jnp.dot(
-            pair, weight[pl.ds(n * columns, 2 * columns), :], preferred_element_type=F32
+            pair, weight[pl.ds(2 * n * columns, 2 * columns), :], preferred_element_type=F32
         )
         total = part if total is None else total + part
     mixed[...] = total.astype(BF)
@@ -400,18 +402,22 @@
         name="near_attention",
     )(tokens, query_weight, far, near, kv1, up, low, high)
 
+    chips = lax.axis_size("tp") // 2
     merged = pl.pallas_call(
         merge_kernel,
         in_specs=[whole()] * 3,
         out_specs=whole(),
-        out_shape=vmem((length, columns)),
+        out_shape=vmem((chips, length, columns)),
         scratch_shapes=[scratch, scratch],
         cost_estimate=cost(1 << 20, 1 << 19),
         compiler_params=room(2),
         name="merge",
     )(parts3, out12, lse12)
 
-    gathered = lax.all_gather(merged, "tp", axis=0, tiled=False)
+    lines = [[2 * n + core for n in range(chips)] for core in range(2)]
+    gathered = lax.all_to_all(merged, "tp", 0, 0, axis_index_groups=lines, tiled=True)
+    cores = [[2 * n, 2 * n + 1] for n in range(chips)]
+    gathered = lax.all_gather(gathered, "tp", axis=0, axis_index_groups=cores)
     return pl.pallas_call(
         output_kernel,
         in_specs=[whole()] * 2,

time: 70 us -> 69.3 us (0.990)
    all_gather x1, blocking collectives: 17.8 us -> 7.69 us  [per_device(): gathered = lax.all_gather(gathered, 'tp', axis=0, axis_index_groups=cores)]
    all_to_all x0 -> x1, blocking collectives: none -> 9.35 us  [per_device(): lax.all_to_all(merged, 'tp', 0, 0, axis_index_groups=lines, tiled=True)]
where the time goes in v4:
time: 69.3 us; the launch traced here: 68.9 us
  blocking collectives  31.6 us (46%)
  starting transfers between devices  17 us (25%)
  Pallas kernels  12.8 us (18%)
  waiting for transfers between devices  7.46 us (11%)
    all_to_all x1, blocking collectives, per_device(): lax.all_to_all(packed, 'sp', 0, 0, axis_index_groups=groups, tiled=True)  14.5 us
    all_to_all x1, blocking collectives, per_device(): lax.all_to_all(merged, 'tp', 0, 0, axis_index_groups=lines, tiled=True)  9.35 us
    all_gather x1, blocking collectives, per_device(): gathered = lax.all_gather(gathered, 'tp', axis=0, axis_index_groups=cores)  7.69 us
    all_to_all x1, starting transfers between devices, per_device(): lax.all_to_all(back, 'sp', 0, 0, axis_index_groups=groups, tiled=True)  6.45 us
    ppermute x1, starting transfers between devices, per_device(): halo3 = lax.ppermute(kv3, 'sp', route)  5.21 us
    ppermute x1, waiting for transfers between devices, per_device(): high = lax.ppermute(down, 'sp', [(s + 1, s) for s in range(devices - 1)])  5.08 us
    pallas_call x1, Pallas kernels, per_device(): pl.pallas_call(functools.partial(near_attention_kernel, devices), in_spec...  4.26 us
    pallas_call x1, Pallas kernels, per_device(): pl.pallas_call(edges_kernel, in_specs=[hbm] * 6, out_specs=[whole()] * le...  3.74 us
  transfers between devices with their start and end apart: 4, of which 2 were waited for; matrix products, arithmetic and copies ran while one was open for 0% of the time, Pallas kernels for 12%

profile of v4, /device:TPU:249, one launch (start us, length us, event | category | flops | bytes accessed | tf_op | source)
XLA Modules:
  0.0 68.9 jit_solution(7899271138891505951)
XLA Ops:
  0.0 2.2 %far_keys_values.1.kv3 = bf16[2,256,128]{2,1,0:T(8,128)(2,1)S(1)} custom-call(bf16[256,2048]{1,0:T(8,128)(2,1)} %tok.5, bf16[3,2048,128]{2,1,0:T(8,128)(2,1)} %wk.3, bf16[3,2048,128]{2,1,0:T(8,128)(2,1)} %wv.3, f32[96,512]{1,0:T(8,128)} %constant.4.clone.far, f32[2,256,128]{2,1,0:T(8,128)} %constant.5.clone.near), custom_call_target="tpu_custom_call" | custom-call | flops 268435456 | bytes 2097152 | tf_op jit(solution)/shard_map/far_keys_values/pallas_call | solution.py:327
  2.2 5.2 %collective-permute-start = (bf16[2,256,128]{2,1,0:T(8,128)(2,1)S(1)}, bf16[2,256,128]{2,1,0:T(8,128)(2,1)S(1)}, u32[]{:S(2)}, u32[]{:S(2)}) collective-permute-start(bf16[2,256,128]{2,1,0:T(8,128)(2,1)S(1)} %far_keys_values.1.kv3), channel_id=1, source_target_pairs={{32,96},{40,104},{48,112},{56,120},{64,0},{72,8},{80,16},{88,24},{... | collective-permute-start | bytes 393224 | tf_op jit(solution)/shard_map/ppermute | solution.py:345
  7.4 3.7 %projections.1 = (bf16[256,128]{1,0:T(8,128)(2,1)S(1)}, bf16[2,256,128]{2,1,0:T(8,128)(2,1)S(1)}, bf16[2,320,128]{2,1,0:T(8,128)(2,1)S(1)}, bf16[2,320,128]{2,1,0:T(8,128)(2,1)S(1)}) custom-call(bf16[256,2048]{1,0:T(8,128)(2,1)} %tok.5, bf16[3,2048,128]{2,1,0:T(8,128)(2,1)} %wq.3, bf16[3,2048,128]{2,1,0:T(8,128)(2,1)} %wk.3, bf16[3,2048,128]{2,1,0:T(8,128)(2,1)} %wv.3, ...), custom_call_target="tpu_custom_call" | custom-call | flops 671088640 | bytes 4194304 | tf_op jit(solution)/shard_map/projections/pallas_call | solution.py:354
  11.2 0.0 collective-permute-done.halo3
  11.2 14.5 %all_to_all.15.parts = bf16[8,160,128]{2,1,0:T(8,128)(2,1)S(1)} all-to-all(bf16[8,160,128]{2,1,0:T(8,128)(2,1)S(1)} %pack.1), channel_id=1, replica_groups={{0,8,16,24,32,40,48,56},{64,72,80,88,96,104,112,120},{128,136,144,152,1..., dimensions={0} | all-to-all | bytes 655360 | tf_op jit(solution)/shard_map/all_to_all | solution.py:380
  25.7 1.4 %far_attention.1 = bf16[8,64,128]{2,1,0:T(8,128)(2,1)} custom-call(bf16[8,160,128]{2,1,0:T(8,128)(2,1)S(1)} %all_to_all.15.parts), custom_call_target="tpu_custom_call" | custom-call | flops 134217728 | bytes 524288 | tf_op jit(solution)/shard_map/far_attention/pallas_call | solution.py:382
  27.1 6.4 %all-to-all-start.1 = ((bf16[8,64,128]{2,1,0:T(8,128)(2,1)}), bf16[8,64,128]{2,1,0:T(8,128)(2,1)S(1)}, u32[]{:S(2)}, u32[]{:S(2)}) async-start(bf16[8,64,128]{2,1,0:T(8,128)(2,1)} %far_attention.1), calls=%async_computation.1 | async-start | bytes 262144 | tf_op jit(solution)/shard_map/all_to_all | solution.py:391
  33.5 3.4 %collective-permute-start.1 = (bf16[2,320,128]{2,1,0:T(8,128)(2,1)S(1)}, bf16[2,320,128]{2,1,0:T(8,128)(2,1)S(1)}, u32[]{:S(2)}, u32[]{:S(2)}) collective-permute-start(bf16[2,320,128]{2,1,0:T(8,128)(2,1)S(1)} %get-tuple-element.13.up), channel_id=1, source_target_pairs={{0,8},{8,16},{16,24},{24,32},{32,40},{40,48},{48,56},{56,64},{64,7... | collective-permute-start | bytes 491528 | tf_op jit(solution)/shard_map/ppermute | solution.py:366
  37.0 1.9 %collective-permute-start.2 = (bf16[2,320,128]{2,1,0:T(8,128)(2,1)S(1)}, bf16[2,320,128]{2,1,0:T(8,128)(2,1)S(1)}, u32[]{:S(2)}, u32[]{:S(2)}) collective-permute-start(bf16[2,320,128]{2,1,0:T(8,128)(2,1)S(1)} %get-tuple-element.14), channel_id=1, source_target_pairs={{8,0},{16,8},{24,16},{32,24},{40,32},{48,40},{56,48},{64,56},{72,6... | collective-permute-start | bytes 491528 | tf_op jit(solution)/shard_map/ppermute | solution.py:367
  38.9 2.4 %collective-permute-done.1.low = bf16[2,320,128]{2,1,0:T(8,128)(2,1)S(1)} collective-permute-done((bf16[2,320,128]{2,1,0:T(8,128)(2,1)S(1)}, bf16[2,320,128]{2,1,0:T(8,128)(2,1)S(1)}, u32[]{:S(2)}, u32[]{:S(2)}) %collective-permute-start.1) | collective-permute-done | bytes 163872 | tf_op jit(solution)/shard_map/ppermute | solution.py:366
  41.3 5.1 %collective-permute-done.2.high = bf16[2,320,128]{2,1,0:T(8,128)(2,1)S(1)} collective-permute-done((bf16[2,320,128]{2,1,0:T(8,128)(2,1)S(1)}, bf16[2,320,128]{2,1,0:T(8,128)(2,1)S(1)}, u32[]{:S(2)}, u32[]{:S(2)}) %collective-permute-start.2) | collective-permute-done | bytes 163872 | tf_op jit(solution)/shard_map/ppermute | solution.py:367
  46.4 4.3 %near_attention.1 = (f32[256,128]{1,0:T(8,128)S(1)}, f32[256,128]{1,0:T(8,128)S(1)}) custom-call(bf16[256,2048]{1,0:T(8,128)(2,1)} %tok.5, bf16[3,2048,128]{2,1,0:T(8,128)(2,1)} %wq.3, f32[96,512]{1,0:T(8,128)} %constant.4.clone.far, f32[2,256,128]{2,1,0:T(8,128)} %constant.5.clone.near, bf16[2,256,128]{2,1,0:T(8,128)(2,1)S(1)} %get-tuple-element.12.kv1, ...), custom_call_target="tpu_custom_call" | custom-call | flops 268435456 | bytes 1048576 | tf_op jit(solution)/shard_map/near_attention/pallas_call | solution.py:393
  50.6 0.0 copy-start
  50.7 0.0 all-to-all-done.1.parts
  50.7 0.2 merge.1
  50.9 9.3 %all_to_all.16 = bf16[4,256,128]{2,1,0:T(8,128)(2,1)S(1)} all-to-all(bf16[4,256,128]{2,1,0:T(8,128)(2,1)S(1)} %merge.1), channel_id=1, replica_groups={{0,2,4,6},{1,3,5,7},{8,10,12,14},{9,11,13,15},{16,18,20,22},{17,19,21,2..., dimensions={0} | all-to-all | bytes 524288 | tf_op jit(solution)/shard_map/all_to_all | solution.py:418
  60.2 7.7 %all-gather = bf16[8,256,128]{2,1,0:T(8,128)(2,1)S(1)} all-gather(bf16[4,256,128]{2,1,0:T(8,128)(2,1)S(1)} %all_to_all.16), channel_id=2, replica_groups={{0,1},{2,3},{4,5},{6,7},{8,9},{10,11},{12,13},{14,15},{16,17},{18,19},{..., dimensions={0}, use_global_device_ids=true | all-gather | bytes 786432 | tf_op jit(solution)/shard_map/all_gather | solution.py:420
  67.9 0.0 copy-done
  67.9 1.0 %output.1 = bf16[256,256]{1,0:T(8,128)(2,1)} custom-call(bf16[2,4,256,128]{3,2,1,0:T(8,128)(2,1)S(1)} %bitcast.1, bf16[1024,256]{1,0:T(8,128)(2,1)S(1)} %copy-done), custom_call_target="tpu_custom_call" | custom-call | flops 134217728 | bytes 1048576 | tf_op jit(solution)/shard_map/output/pallas_call | solution.py:421
  (1 shorter events, 0.0 us)
Async XLA Ops:
  2.2 9.0 %collective-permute-start = (bf16[2,256,128]{2,1,0:T(8,128)(2,1)S(1)}, bf16[2,256,128]{2,1,0:T(8,128)(2,1)S(1)}, u32[]{:S(2)}, u32[]{:S(2)}) collective-permute-start(bf16[2,256,128]{2,1,0:T(8,128)(2,1)S(1)} %far_keys_values.1.kv3), channel_id=1, source_target_pairs={{32,96},{40,104},{48,112},{56,120},{64,0},{72,8},{80,16},{88,24},{... | collective-permute-start | bytes 393224 | tf_op jit(solution)/shard_map/ppermute | solution.py:345
  27.1 23.6 %all-to-all-start.1 = ((bf16[8,64,128]{2,1,0:T(8,128)(2,1)}), bf16[8,64,128]{2,1,0:T(8,128)(2,1)S(1)}, u32[]{:S(2)}, u32[]{:S(2)}) async-start(bf16[8,64,128]{2,1,0:T(8,128)(2,1)} %far_attention.1), calls=%async_computation.1 | async-start | bytes 262144 | tf_op jit(solution)/shard_map/all_to_all | solution.py:391
  33.5 7.7 %collective-permute-start.1 = (bf16[2,320,128]{2,1,0:T(8,128)(2,1)S(1)}, bf16[2,320,128]{2,1,0:T(8,128)(2,1)S(1)}, u32[]{:S(2)}, u32[]{:S(2)}) collective-permute-start(bf16[2,320,128]{2,1,0:T(8,128)(2,1)S(1)} %get-tuple-element.13.up), channel_id=1, source_target_pairs={{0,8},{8,16},{16,24},{24,32},{32,40},{40,48},{48,56},{56,64},{64,7... | collective-permute-start | bytes 491528 | tf_op jit(solution)/shard_map/ppermute | solution.py:366
  37.0 9.4 %collective-permute-start.2 = (bf16[2,320,128]{2,1,0:T(8,128)(2,1)S(1)}, bf16[2,320,128]{2,1,0:T(8,128)(2,1)S(1)}, u32[]{:S(2)}, u32[]{:S(2)}) collective-permute-start(bf16[2,320,128]{2,1,0:T(8,128)(2,1)S(1)} %get-tuple-element.14), channel_id=1, source_target_pairs={{8,0},{16,8},{24,16},{32,24},{40,32},{48,40},{56,48},{64,56},{72,6... | collective-permute-start | bytes 491528 | tf_op jit(solution)/shard_map/ppermute | solution.py:367
  50.6 17.3 %copy-start = (bf16[1024,256]{1,0:T(8,128)(2,1)S(1)}, bf16[1024,256]{1,0:T(8,128)(2,1)}, u32[]{:S(2)}) copy-start(bf16[1024,256]{1,0:T(8,128)(2,1)} %weight.1) | copy-start | bytes 1572868
